TPU v7x, 32 devices: a whole 2x2x4 slice. The times are simulated.
32 devices in a mesh: ep: 16 (over z, y, x), tp: 2 (over core).
Axes of the slice: x: 2, y: 2, z: 4, core: 2. Of those that a mesh axis runs over, the one named last changes fastest.
Arguments:
- tokens: bfloat16 [256, 2048], P('ep'), may hold values from -6 to 6
- norm_attn: float32 [2048], replicated, may hold values from 0.1 to 1.9
- w_query: bfloat16 [2048, 2048], P(None, 'tp'), may hold values from -0.125 to 0.125
- w_key: bfloat16 [2048, 256], P(None, 'tp'), may hold values from -0.125 to 0.125
- w_value: bfloat16 [2048, 256], P(None, 'tp'), may hold values from -0.125 to 0.125
- w_out: bfloat16 [2048, 2048], P('tp'), may hold values from -0.125 to 0.125
- attn_bias: float32 [32], P('tp'), may hold values from -7 to -1
- cache_keys: bfloat16 [256, 1024, 256], P('ep', None, 'tp'), may hold values from -6 to 6
- cache_values: bfloat16 [256, 1024, 256], P('ep', None, 'tp'), may hold values from -6 to 6
- lengths: int32 [256], P('ep'), may hold values from 256 to 1024
- norm_ffn: float32 [2048], replicated, may hold values from 0.1 to 1.9
- expert_gate: bfloat16 [2048, 57344], P(None, ('ep', 'tp')), may hold values from -0.125 to 0.125
- expert_up: bfloat16 [2048, 57344], P(None, ('ep', 'tp')), may hold values from -0.125 to 0.125
- expert_down: bfloat16 [57344, 2048], P(('ep', 'tp')), may hold values from -0.0625 to 0.0625
- dense_gate_w: bfloat16 [2048, 7168], P(None, 'ep'), may hold values from -0.125 to 0.125
- dense_up_w: bfloat16 [2048, 7168], P(None, 'ep'), may hold values from -0.125 to 0.125
- dense_down_w: bfloat16 [7168, 2048], P('ep'), may hold values from -0.0625 to 0.0625
- dense_mix: bfloat16 [2048], replicated, may hold values from -0.125 to 0.125
- routes: int32 [256, 2], P(('ep', 'tp')), may hold values from 0 to 7, all different within a row; in each aligned block of 8 rows (0 to 7, 8 to 15, ...) at most 3 rows name the same one
- route_weights: bfloat16 [256, 2], P(('ep', 'tp')), may hold values from 0.19921875 to 1
Outputs:
- layer_out: bfloat16 [256, 2048], P(('ep', 'tp'))
- new_keys: bfloat16 [256, 256], P('ep', 'tp')
- new_values: bfloat16 [256, 256], P('ep', 'tp')
Inputs may be any that keep to these rules, and one draw needn't show every extreme that they name: `routes`: in each aligned block of 8 rows (the rows of one device) no expert is named by more than 3 rows, a bound that some block reaches; a row names 2 different experts.
All inputs are finite; a program needn't handle non-finite values.
Results may differ from a plain program's by a relative error of at most 0.015.
Values may be sent and summed in bfloat16 or wider, within the bound.
No kernel may reach another device: no remote copies, remote signals or barrier semaphores. Data moves between devices by JAX's collectives and lax.ppermute only.
A program may use at most 128 MiB of HBM per device.

v0:
```python
import functools
import math

import jax
import jax.numpy as jnp
from jax import lax
from jax.experimental import pallas as pl
from jax.experimental.pallas import tpu as pltpu
from jax.sharding import PartitionSpec as P

HEAD_DIM = 64
EXPERTS = 8
LANES = 128
EPSILON = 1e-06
FETCH_FLOPS = 200
F32 = jnp.float32
BF16 = jnp.bfloat16


HBM = pl.BlockSpec(memory_space=pltpu.HBM)
VMEM = pl.BlockSpec(memory_space=pltpu.VMEM)


def in_hbm(*arrays):
    return [pltpu.with_memory_space_constraint(array, pltpu.HBM) for array in arrays]


def split_of(total, most):
    for pieces in range(most, 0, -1):
        if total % (pieces * 256) == 0:
            return pieces
    return 1


def normed_block(widened, gain):
    scale = lax.rsqrt(jnp.mean(widened * widened, axis=-1, keepdims=True) + EPSILON)
    return (widened * scale * gain).astype(BF16)


def attention_kernel(
    row_count, group,
    lengths_hbm, tokens_hbm, gain_hbm, bias_hbm,
    wq_hbm, wk_hbm, wv_hbm, wo_hbm, keys_hbm, values_hbm,
    keep_ref, send_ref, new_keys_ref, new_values_ref,
    lengths_ref, tokens_ref, gain_ref, bias_ref,
    wq, wk, wv, wo, keys, values, queries, mixed, later, partial,
    sem_small, sem_q, sem_kv, sem_k, sem_v, sem_o,
):
    seqs, width = tokens_ref.shape
    cache = keys.shape[1]
    q_width = wq.shape[1]
    heads = q_width // HEAD_DIM
    pairs = heads // 2
    q_parts = sem_q.shape[0]
    o_parts = sem_o.shape[0]
    groups = seqs // group
    q_rows = width // q_parts
    o_rows = q_width // o_parts
    half = 2 * LANES

    def q_copy(i):
        rows = pl.ds(i * q_rows, q_rows)
        return pltpu.make_async_copy(wq_hbm.at[rows], wq.at[rows], sem_q.at[i])

    def o_copy(i):
        rows = pl.ds(i * o_rows, o_rows)
        return pltpu.make_async_copy(wo_hbm.at[rows], wo.at[rows], sem_o.at[i])

    def k_copy(i):
        rows = pl.ds(i * group, group)
        return pltpu.make_async_copy(keys_hbm.at[rows], keys.at[rows], sem_k.at[i])

    def v_copy(i):
        rows = pl.ds(i * group, group)
        return pltpu.make_async_copy(values_hbm.at[rows], values.at[rows], sem_v.at[i])

    small = [
        pltpu.make_async_copy(source, target, sem_small.at[i])
        for i, (source, target) in enumerate((
            (tokens_hbm, tokens_ref), (gain_hbm, gain_ref),
            (lengths_hbm, lengths_ref), (bias_hbm, bias_ref),
        ))
    ]
    for copy in small:
        copy.start()
    copy_wk = pltpu.make_async_copy(wk_hbm, wk, sem_kv.at[0])
    copy_wv = pltpu.make_async_copy(wv_hbm, wv, sem_kv.at[1])
    for i in range(q_parts):
        q_copy(i).start()
    for i in range(groups):
        k_copy(i).start()
        v_copy(i).start()
    copy_wk.start()
    copy_wv.start()
    for i in range(o_parts):
        o_copy(i).start()

    later_rows = lax.broadcasted_iota(jnp.int32, (2 * half, half), 0) % half
    later_cols = lax.broadcasted_iota(jnp.int32, (2 * half, half), 1)
    later[...] = (later_rows > later_cols).astype(F32).astype(BF16)

    for copy in small:
        copy.wait()
    normed = normed_block(tokens_ref[...].astype(F32), gain_ref[...])
    query = jnp.zeros((seqs, q_width), F32)
    for i in range(q_parts):
        q_copy(i).wait()
        query += jnp.dot(
            normed[:, i * q_rows:(i + 1) * q_rows],
            wq[i * q_rows:(i + 1) * q_rows, :],
            preferred_element_type=F32,
        )
    query = query.astype(BF16).astype(F32)

    lane = lax.broadcasted_iota(jnp.int32, (seqs, LANES), 1)
    low = lane < HEAD_DIM
    for pair in range(pairs):
        both = query[:, pair * LANES:(pair + 1) * LANES]
        turned = pltpu.roll(both, HEAD_DIM, 1)
        if 2 * pair < heads // 2:
            first, second = jnp.where(low, both, 0.0), jnp.where(low, turned, 0.0)
        else:
            first, second = jnp.where(low, 0.0, turned), jnp.where(low, 0.0, both)
        queries[pl.ds(2 * pair, seqs, stride=heads), :] = first
        queries[pl.ds(2 * pair + 1, seqs, stride=heads), :] = second

    rows = group * heads
    head_of = lax.broadcasted_iota(jnp.int32, (heads, 1), 0)
    bias = jnp.zeros((heads, 1), F32)
    for head in range(heads):
        bias = jnp.where(head_of == head, bias_ref[head], bias)
    bias = jnp.concatenate([bias] * group, axis=0)
    seq_of = lax.broadcasted_iota(jnp.int32, (rows, 1), 0) // heads
    place = lax.broadcasted_iota(jnp.int32, (rows, half), 1)
    blocks = cache // half

    def attend(step, carry):
        k_copy(step).wait()
        first = step * group
        scores = []
        for s in range(group):
            q_seq = queries[pl.ds(pl.multiple_of((first + s) * heads, heads), heads), :]
            scores.append(
                lax.dot_general(
                    q_seq.astype(BF16), keys[first + s], (((1,), (1,)), ((), ())),
                    preferred_element_type=F32,
                )
            )
        scores = jnp.concatenate(scores, axis=0)
        length = jnp.zeros((rows, 1), jnp.int32)
        for s in range(group):
            length = jnp.where(seq_of == s, lengths_ref[first + s], length)
        opened, pieces, heads_first = [], [], []
        for n in range(blocks):
            z = scores[:, n * half:(n + 1) * half] * HEAD_DIM ** (-0.5) + bias
            shared = jnp.log(1.0 + jnp.exp(-jnp.abs(z)))
            visible = place + n * half < length
            kept = jnp.where(visible, -(jnp.maximum(z, 0.0) + shared), 0.0)
            opened.append(jnp.where(visible, jnp.minimum(z, 0.0) - shared, -jnp.inf))
            coarse = kept.astype(BF16)
            fine = (kept - coarse.astype(F32)).astype(BF16)
            pieces.append(jnp.concatenate([coarse, fine], axis=1))
            heads_first.append(kept[:, 0:1])
        after = jnp.dot(
            jnp.concatenate(pieces, axis=0), later[...], preferred_element_type=F32
        )
        beyond = jnp.zeros((rows, 1), F32)
        weights = [None] * blocks
        for n in reversed(range(blocks)):
            within = after[n * rows:(n + 1) * rows]
            weights[n] = jnp.exp(opened[n] + within + beyond).astype(BF16)
            beyond = beyond + within[:, 0:1] + heads_first[n]
        weights = jnp.concatenate(weights, axis=1)
        v_copy(step).wait()
        for s in range(group):
            mixed[pl.ds(pl.multiple_of((first + s) * heads, heads), heads), :] = jnp.dot(
                weights[s * heads:(s + 1) * heads], values[first + s],
                preferred_element_type=F32,
            )
        return carry

    lax.fori_loop(0, groups, attend, 0)

    copy_wk.wait()
    copy_wv.wait()
    new_keys_ref[...] = jnp.dot(normed, wk[...], preferred_element_type=F32).astype(BF16)
    new_values_ref[...] = jnp.dot(normed, wv[...], preferred_element_type=F32).astype(BF16)

    joined = []
    for pair in range(pairs):
        first = mixed[pl.ds(2 * pair, seqs, stride=heads), :]
        second = mixed[pl.ds(2 * pair + 1, seqs, stride=heads), :]
        if 2 * pair < heads // 2:
            second = pltpu.roll(second, HEAD_DIM, 1)
        else:
            first = pltpu.roll(first, HEAD_DIM, 1)
        joined.append(jnp.where(low, first, second).astype(BF16))
    heads_out = jnp.concatenate(joined, axis=1)
    total = jnp.zeros((seqs, width), F32)
    for i in range(o_parts):
        o_copy(i).wait()
        total += jnp.dot(
            heads_out[:, i * o_rows:(i + 1) * o_rows],
            wo[i * o_rows:(i + 1) * o_rows, :],
            preferred_element_type=F32,
        )
    partial[...] = total
    own = lax.axis_index("tp") * row_count
    other = seqs - row_count - own
    keep_ref[...] = partial[pl.ds(pl.multiple_of(own, 8), row_count), :].astype(BF16)
    send_ref[...] = partial[pl.ds(pl.multiple_of(other, 8), row_count), :].astype(BF16)


def attention(tokens, norm_attn, w_query, w_key, w_value, w_out, attn_bias,
              cache_keys, cache_values, lengths, row_count):
    seqs, width = tokens.shape
    q_width = w_query.shape[1]
    kv_width = w_key.shape[1]
    heads = q_width // HEAD_DIM
    group = 4 if seqs % 4 == 0 else 1
    q_parts = split_of(width, 4)
    o_parts = split_of(q_width, 4)
    dma = pltpu.SemaphoreType.DMA
    half = jax.ShapeDtypeStruct((row_count, width), BF16)
    kv = jax.ShapeDtypeStruct((seqs, kv_width), BF16)
    return pl.pallas_call(
        functools.partial(attention_kernel, row_count, group),
        out_shape=(half, half, kv, kv),
        in_specs=[HBM] * 10,
        out_specs=(VMEM,) * 4,
        scratch_shapes=[
            pltpu.SMEM(lengths.shape, jnp.int32),
            pltpu.VMEM(tokens.shape, BF16),
            pltpu.VMEM((1, width), F32),
            pltpu.SMEM(attn_bias.shape, F32),
            pltpu.VMEM(w_query.shape, BF16),
            pltpu.VMEM(w_key.shape, BF16),
            pltpu.VMEM(w_value.shape, BF16),
            pltpu.VMEM(w_out.shape, BF16),
            pltpu.VMEM(cache_keys.shape, BF16),
            pltpu.VMEM(cache_values.shape, BF16),
            pltpu.VMEM((seqs * heads, LANES), F32),
            pltpu.VMEM((seqs * heads, LANES), F32),
            pltpu.VMEM((4 * LANES, 2 * LANES), BF16),
            pltpu.VMEM((seqs, width), F32),
            dma((4,)), dma((q_parts,)), dma((2,)), dma((seqs // group,)), dma((seqs // group,)),
            dma((o_parts,)),
        ],
        compiler_params=pltpu.CompilerParams(vmem_limit_bytes=36 * 2**20),
        name="attention",
    )(*in_hbm(lengths, tokens, norm_attn.reshape(1, -1), attn_bias, w_query, w_key,
              w_value, w_out, cache_keys, cache_values))


def middle_kernel(row_count, tokens_ref, keep_ref, got_ref, gain_ref, mix_ref, routes_ref,
                  weights_ref, out_ref, middle_ref, wide):
    width = keep_ref.shape[1]
    wide[...] = tokens_ref[...].astype(F32)
    own = pl.multiple_of(lax.axis_index("tp") * row_count, 8)
    attn_sum = keep_ref[...].astype(F32) + got_ref[...].astype(F32)
    middle = (wide[pl.ds(own, row_count), :] + attn_sum).astype(BF16)
    middle_ref[...] = middle
    normed = normed_block(middle.astype(F32), gain_ref[...])
    out_ref[:, :width] = normed
    dot = jnp.sum(normed.astype(F32) * mix_ref[...].astype(F32), axis=-1, keepdims=True)
    gate = 1.0 / (1.0 + jnp.exp(-dot))
    coarse = gate.astype(BF16).astype(F32)
    lane = lax.broadcasted_iota(jnp.int32, (row_count, LANES), 1)
    extra = jnp.where(lane == EXPERTS, coarse, 0.0)
    extra = jnp.where(lane == EXPERTS + 1, gate - coarse, extra)
    for choice in range(routes_ref.shape[1]):
        extra += jnp.where(
            lane == routes_ref[:, choice:choice + 1],
            weights_ref[:, choice:choice + 1].astype(F32), 0.0,
        )
    out_ref[:, width:] = extra.astype(BF16)


def make_middle(tokens, keep, got, norm_ffn, dense_mix, routes, route_weights):
    row_count, width = keep.shape
    return pl.pallas_call(
        functools.partial(middle_kernel, row_count),
        out_shape=(
            jax.ShapeDtypeStruct((row_count, width + LANES), BF16),
            jax.ShapeDtypeStruct((row_count, width), BF16),
        ),
        in_specs=[VMEM] * 7,
        out_specs=(VMEM,) * 2,
        scratch_shapes=[pltpu.VMEM(tokens.shape, F32)],
        compiler_params=pltpu.CompilerParams(vmem_limit_bytes=4 * 2**20),
        name="middle",
    )(tokens, keep, got, norm_ffn.reshape(1, -1), dense_mix.reshape(1, -1), routes,
      route_weights)


def units_part(units):
    return pl.ds(pl.multiple_of(lax.axis_index("tp") * units, 8), units)


def fetch_all(copies, sems):
    copies = [
        pltpu.make_async_copy(source, target, sems.at[i])
        for i, (source, target) in enumerate(copies)
    ]
    for copy in copies:
        copy.start()
    for copy in copies:
        copy.wait()


def fetch_up_kernel(after_hbm, gate_hbm, up_hbm, dense_gate_hbm, dense_up_hbm, wide, dense, sems):
    hidden, _, block = wide.shape
    part = units_part(dense.shape[1])
    copies = []
    if block == gate_hbm.shape[1]:
        copies += [(gate_hbm, wide.at[0]), (up_hbm, wide.at[1])]
    else:
        block //= 2
        for i in range(hidden):
            cols = pl.ds(i * block, block)
            copies.append((gate_hbm.at[:, cols], wide.at[i, :, pl.ds(0, block)]))
            copies.append((up_hbm.at[:, cols], wide.at[i, :, pl.ds(block, block)]))
    copies.append((dense_gate_hbm.at[part], dense.at[0]))
    copies.append((dense_up_hbm.at[part], dense.at[1]))
    fetch_all(copies, sems)


def fetch_down_kernel(after_hbm, down_hbm, dense_down_hbm, down, dense, sems):
    pieces = sems.shape[0] // 2
    rows = down.shape[0] // pieces
    dense_rows = dense.shape[0] // pieces
    first = units_part(dense.shape[0]).start
    copies = []
    for i in range(pieces):
        part = pl.ds(i * rows, rows)
        copies.append((down_hbm.at[part], down.at[part]))
        source = pl.ds(pl.multiple_of(first + i * dense_rows, 8), dense_rows)
        copies.append((dense_down_hbm.at[source], dense.at[pl.ds(i * dense_rows, dense_rows)]))
    fetch_all(copies, sems)


def fetch_call(kernel, after, arrays, shapes, copies):
    size = sum(2 * math.prod(shape) for shape in shapes)
    return pl.pallas_call(
        kernel,
        out_shape=tuple(pltpu.VMEM(shape, BF16) for shape in shapes),
        in_specs=[HBM] * (1 + len(arrays)),
        out_specs=(VMEM,) * len(shapes),
        scratch_shapes=[pltpu.SemaphoreType.DMA((copies,))],
        cost_estimate=pl.CostEstimate(
            flops=FETCH_FLOPS * size, bytes_accessed=size, transcendentals=0
        ),
        compiler_params=pltpu.CompilerParams(vmem_limit_bytes=2**20),
    )(after, *in_hbm(*arrays))


def fetch_weights(after_first, after_second, expert_gate, expert_up, expert_down, dense_gate_w,
                  dense_up_w, dense_down_w):
    width, units = expert_gate.shape
    wide = (units // 256, width, 512) if units % 512 == 256 else (2, width, units)
    dense_units = dense_gate_w.shape[1] // lax.axis_size("tp")
    pieces = 4 if units % 64 == 0 and dense_units % 32 == 0 else 1
    down, dense_down = fetch_call(
        fetch_down_kernel, after_first, (expert_down, dense_down_w),
        ((units, width), (dense_units, width)), 2 * pieces,
    )
    wide, dense = fetch_call(
        fetch_up_kernel, after_second,
        (expert_gate, expert_up, dense_gate_w.T, dense_up_w.T),
        (wide, (2, dense_units, width)), 2 * max(wide[0], 1) + 2,
    )
    return wide, dense, down, dense_down


def ffn_kernel(members, out_block, rows_ref, wide, dense, down, dense_down, own_ref, other_ref,
               hidden_ref):
    count, padded = rows_ref.shape
    width = padded - LANES
    units = down.shape[0]
    hidden, _, block = wide.shape
    device = lax.axis_index("ep") * lax.axis_size("tp") + lax.axis_index("tp")
    expert = device // members
    extra = rows_ref[:, width:].astype(F32)
    lane = lax.broadcasted_iota(jnp.int32, extra.shape, 1)
    share = jnp.sum(jnp.where(lane == expert, extra, 0.0), axis=-1, keepdims=True)
    gated = (lane == EXPERTS) | (lane == EXPERTS + 1)
    mix = jnp.sum(jnp.where(gated, extra, 0.0), axis=-1, keepdims=True)

    def activate(gate, up, scale):
        return (gate / (1.0 + jnp.exp(-gate)) * up * scale).astype(BF16)

    rows = rows_ref[:, :width]
    if block == units:
        gate, up = (jnp.dot(rows, wide[i], preferred_element_type=F32) for i in range(2))
        hidden_ref[...] = activate(gate, up, share)
    else:
        block //= 2
        for i in range(hidden):
            both = jnp.dot(rows, wide[i], preferred_element_type=F32)
            hidden_ref[:, i * block:(i + 1) * block] = activate(
                both[:, :block], both[:, block:], share
            )
    dims = (((1,), (1,)), ((), ()))
    gate, up = (
        lax.dot_general(rows, dense[i], dims, preferred_element_type=F32) for i in range(2)
    )
    dense_hidden = activate(gate, up, mix)
    for first in range(0, width, out_block):
        cols = slice(first, first + out_block)
        total = jnp.dot(hidden_ref[...], down[:, cols], preferred_element_type=F32)
        total += jnp.dot(dense_hidden, dense_down[:, cols], preferred_element_type=F32)
        own_ref[:, cols] = total[:count // 2]
        other_ref[:, cols] = total[count // 2:].astype(BF16)


def feed_forward(rows, weights, members):
    count, padded = rows.shape
    width = padded - LANES
    units = weights[2].shape[0]
    return pl.pallas_call(
        functools.partial(ffn_kernel, members, 512 if width % 512 == 0 else width),
        out_shape=(
            jax.ShapeDtypeStruct((count // 2, width), F32),
            jax.ShapeDtypeStruct((count // 2, width), BF16),
        ),
        in_specs=[VMEM] * 5,
        out_specs=(VMEM,) * 2,
        scratch_shapes=[pltpu.VMEM((count, units), BF16)],
        cost_estimate=pl.CostEstimate(
            flops=6 * count * width * units, bytes_accessed=0, transcendentals=0
        ),
        compiler_params=pltpu.CompilerParams(vmem_limit_bytes=16 * 2**20),
        name="feed_forward",
    )(rows, *weights)


def phases_of(n_ep):
    bits = [1 << b for b in range(n_ep.bit_length() - 1)]
    phases = []
    while len(bits) >= 2:
        high, low = bits.pop(), bits.pop()
        phases += [(low, high), (high, low)]
    return phases + [(bit, bit) for bit in bits]


def exchange(array, masks, n_ep, n_tp):
    pairs = [
        (ep * n_tp + tp, (ep ^ masks[tp % 2]) * n_tp + tp)
        for ep in range(n_ep) for tp in range(n_tp)
    ]
    return lax.ppermute(array, ("ep", "tp"), pairs)


def swap(array, n_tp):
    return lax.ppermute(array, "tp", [(i, i ^ 1) for i in range(n_tp)])


def layer(
    tokens, norm_attn, w_query, w_key, w_value, w_out, attn_bias, cache_keys, cache_values,
    lengths, norm_ffn, expert_gate, expert_up, expert_down, dense_gate_w, dense_up_w,
    dense_down_w, dense_mix, routes, route_weights,
):
    n_ep, n_tp = lax.axis_size("ep"), lax.axis_size("tp")
    row_count = tokens.shape[0] // n_tp
    keep, send, new_keys, new_values = attention(
        tokens, norm_attn, w_query, w_key, w_value, w_out, attn_bias, cache_keys,
        cache_values, lengths, row_count,
    )
    rows, middle = make_middle(
        tokens, keep, swap(send, n_tp), norm_ffn, dense_mix, routes, route_weights
    )
    phases = phases_of(n_ep)
    held = []
    for masks in phases:
        held.append(rows)
        got = exchange(rows, masks, n_ep, n_tp)
        rows = jnp.concatenate([rows, got], axis=0)
    weights = fetch_weights(
        held[-2], held[-1], expert_gate, expert_up, expert_down, dense_gate_w, dense_up_w,
        dense_down_w,
    )
    rows = jnp.concatenate([rows, swap(rows, n_tp)], axis=0)
    own, other = feed_forward(rows, weights, n_ep * n_tp // EXPERTS)
    total = own + swap(other, n_tp).astype(F32)
    for masks in reversed(phases):
        half = total.shape[0] // 2
        got = exchange(total[half:].astype(BF16), masks, n_ep, n_tp)
        total = total[:half] + got.astype(F32)
    layer_out = (middle.astype(F32) + total).astype(BF16)
    return layer_out, new_keys, new_values


def solution(mesh):
    placed = (
        P("ep", None),
        P(),
        P(None, "tp"),
        P(None, "tp"),
        P(None, "tp"),
        P("tp", None),
        P("tp"),
        P("ep", None, "tp"),
        P("ep", None, "tp"),
        P("ep"),
        P(),
        P(None, ("ep", "tp")),
        P(None, ("ep", "tp")),
        P(("ep", "tp"), None),
        P(None, "ep"),
        P(None, "ep"),
        P("ep", None),
        P(),
        P(("ep", "tp"), None),
        P(("ep", "tp"), None),
    )
    return jax.shard_map(
        layer,
        mesh=mesh,
        in_specs=placed,
        out_specs=(P(("ep", "tp"), None), P("ep", "tp"), P("ep", "tp")),
        check_vma=False,
    )
```

profile of v0, /device:TPU:0, one launch (start us, length us, event | category | flops | bytes accessed | tf_op | source)
XLA Modules:
  0.0 76.9 jit_solution(9436024965396377312)
XLA Ops:
  0.7 11.1 %attention.1 = (bf16[8,2048]{1,0:T(8,128)(2,1)S(1)}, bf16[8,2048]{1,0:T(8,128)(2,1)S(1)}, bf16[16,128]{1,0:T(8,128)(2,1)}, bf16[16,128]{1,0:T(8,128)(2,1)}) custom-call(s32[16]{0:T(128)} %lengths_hbm.1, bf16[16,2048]{1,0:T(8,128)(2,1)} %tokens_ref.1, f32[1,2048]{1,0:T(1,128)} %bitcast.7, f32[16]{0:T(128)} %bias_hbm.1, bf16[2048,1024]{1,0:T(8,128)(2,1)} %wq_hbm.1, ...), custom_call_target="tpu_custom_call" | custom-call | tf_op jit(solution)/shard_map/attention/pallas_call | solution.py:226
  11.8 0.6 collective-permute-start
  12.6 0.7 collective-permute-done.got_ref
  13.5 3.0 %collective-permute-start.1 = (bf16[8,2176]{1,0:T(8,128)(2,1)S(1)}, bf16[8,2176]{1,0:T(8,128)(2,1)S(1)}, u32[]{:S(2)}, u32[]{:S(2)}) collective-permute-start(bf16[8,2176]{1,0:T(8,128)(2,1)S(1)} %get-tuple-element.18), channel_id=1, source_target_pairs={{0,8},{1,17},{2,10},{3,19},{4,12},{5,21},{6,14},{7,23},{8,0},{9,25... | collective-permute-start | bytes 104456 | tf_op jit(solution)/shard_map/ppermute | solution.py:451
  16.5 1.9 %collective-permute-done.1 = bf16[8,2176]{1,0:T(8,128)(2,1)S(1)} collective-permute-done((bf16[8,2176]{1,0:T(8,128)(2,1)S(1)}, bf16[8,2176]{1,0:T(8,128)(2,1)S(1)}, u32[]{:S(2)}, u32[]{:S(2)}) %collective-permute-start.1) | collective-permute-done | bytes 34848 | tf_op jit(solution)/shard_map/ppermute | solution.py:451
  18.4 3.0 %collective-permute-start.2 = (bf16[16,2176]{1,0:T(8,128)(2,1)S(1)}, bf16[16,2176]{1,0:T(8,128)(2,1)S(1)}, u32[]{:S(2)}, u32[]{:S(2)}) collective-permute-start(bf16[16,2176]{1,0:T(8,128)(2,1)S(1)} %pad_maximum_fusion), channel_id=1, source_target_pairs={{0,16},{1,9},{2,18},{3,11},{4,20},{5,13},{6,22},{7,15},{8,24},{9,1... | collective-permute-start | bytes 208904 | tf_op jit(solution)/shard_map/ppermute | solution.py:451
  21.4 2.3 %collective-permute-done.2 = bf16[16,2176]{1,0:T(8,128)(2,1)S(1)} collective-permute-done((bf16[16,2176]{1,0:T(8,128)(2,1)S(1)}, bf16[16,2176]{1,0:T(8,128)(2,1)S(1)}, u32[]{:S(2)}, u32[]{:S(2)}) %collective-permute-start.2) | collective-permute-done | bytes 69664 | tf_op jit(solution)/shard_map/ppermute | solution.py:451
  23.7 2.3 %collective-permute-start.3 = (bf16[32,2176]{1,0:T(8,128)(2,1)S(1)}, bf16[32,2176]{1,0:T(8,128)(2,1)S(1)}, u32[]{:S(2)}, u32[]{:S(2)}) collective-permute-start(bf16[32,2176]{1,0:T(8,128)(2,1)S(1)} %get-tuple-element.35.after_hbm), channel_id=1, source_target_pairs={{0,2},{1,5},{2,0},{3,7},{4,6},{5,1},{6,4},{7,3},{8,10},{9,13},{10,... | collective-permute-start | bytes 417800 | tf_op jit(solution)/shard_map/ppermute | solution.py:451
  26.0 3.5 %collective-permute-done.3 = bf16[32,2176]{1,0:T(8,128)(2,1)S(1)} collective-permute-done((bf16[32,2176]{1,0:T(8,128)(2,1)S(1)}, bf16[32,2176]{1,0:T(8,128)(2,1)S(1)}, u32[]{:S(2)}, u32[]{:S(2)}) %collective-permute-start.3) | collective-permute-done | bytes 139296 | tf_op jit(solution)/shard_map/ppermute | solution.py:451
  29.6 2.5 %collective-permute-start.4 = (bf16[64,2176]{1,0:T(8,128)(2,1)S(1)}, bf16[64,2176]{1,0:T(8,128)(2,1)S(1)}, u32[]{:S(2)}, u32[]{:S(2)}) collective-permute-start(bf16[64,2176]{1,0:T(8,128)(2,1)S(1)} %get-tuple-element.31.after_hbm), channel_id=1, source_target_pairs={{0,4},{1,3},{2,6},{3,1},{4,0},{5,7},{6,2},{7,5},{8,12},{9,11},{10,... | collective-permute-start | bytes 835592 | tf_op jit(solution)/shard_map/ppermute | solution.py:451
  32.0 4.5 %collective-permute-done.4 = bf16[64,2176]{1,0:T(8,128)(2,1)S(1)} collective-permute-done((bf16[64,2176]{1,0:T(8,128)(2,1)S(1)}, bf16[64,2176]{1,0:T(8,128)(2,1)S(1)}, u32[]{:S(2)}, u32[]{:S(2)}) %collective-permute-start.4) | collective-permute-done | bytes 278560 | tf_op jit(solution)/shard_map/ppermute | solution.py:451
  36.7 3.4 %shard_map.212 = (bf16[1792,2048]{1,0:T(8,128)(2,1)S(1)}, bf16[224,2048]{1,0:T(8,128)(2,1)S(1)}) custom-call(bf16[32,2176]{1,0:T(8,128)(2,1)S(1)} %get-tuple-element.35.after_hbm, bf16[1792,2048]{1,0:T(8,128)(2,1)} %down_hbm.1, bf16[448,2048]{1,0:T(8,128)(2,1)} %dense_down_hbm.1), custom_call_target="tpu_custom_call" | custom-call | flops 1651507200 | bytes 8257536 | tf_op jit(solution)/shard_map/pallas_call | solution.py:344
  40.1 6.1 %shard_map.211 = (bf16[7,2048,512]{2,1,0:T(8,128)(2,1)S(1)}, bf16[2,224,2048]{2,1,0:T(8,128)(2,1)S(1)}) custom-call(bf16[64,2176]{1,0:T(8,128)(2,1)S(1)} %get-tuple-element.31.after_hbm, bf16[2048,1792]{1,0:T(8,128)(2,1)} %gate_hbm.1, bf16[2048,1792]{1,0:T(8,128)(2,1)} %up_hbm.1, bf16[448,2048]{1,0:T(8,128)(2,1)} %bitcast.5, bf16[448,2048]{1,0:T(8,128)(2,1)} %bitcast.6), custom_call_target="tpu_custom_call" | custom-call | flops 3303014400 | bytes 16515072 | tf_op jit(solution)/shard_map/pallas_call | solution.py:344
  46.3 6.8 %feed_forward.1 = (f32[128,2048]{1,0:T(8,128)S(1)}, bf16[128,2048]{1,0:T(8,128)(2,1)S(1)}) custom-call(bf16[256,2176]{1,0:T(8,128)(2,1)S(1)} %constant_dynamic-update-slice_fusion.12.rows_ref, bf16[7,2048,512]{2,1,0:T(8,128)(2,1)S(1)} %get-tuple-element.19.wide, bf16[2,224,2048]{2,1,0:T(8,128)(2,1)S(1)} %get-tuple-element.20.dense, ...), custom_call_target="tpu_custom_call" | custom-call | flops 5637144576 | tf_op jit(solution)/shard_map/feed_forward/pallas_call | solution.py:420
  53.7 1.5 %collective-permute-done.6 = bf16[128,2048]{1,0:T(8,128)(2,1)S(1)} collective-permute-done((bf16[128,2048]{1,0:T(8,128)(2,1)S(1)}, bf16[128,2048]{1,0:T(8,128)(2,1)S(1)}, u32[]{:S(2)}, u32[]{:S(2)}) %collective-permute-start.6) | collective-permute-done | bytes 524320 | tf_op jit(solution)/shard_map/ppermute | solution.py:455
  55.3 2.1 %collective-permute-start.7 = (bf16[64,2048]{1,0:T(8,128)(2,1)S(1)}, bf16[64,2048]{1,0:T(8,128)(2,1)S(1)}, u32[]{:S(2)}, u32[]{:S(2)}) collective-permute-start(bf16[64,2048]{1,0:T(8,128)(2,1)S(1)} %slice.56), channel_id=1, source_target_pairs={{0,4},{1,3},{2,6},{3,1},{4,0},{5,7},{6,2},{7,5},{8,12},{9,11},{10,... | collective-permute-start | bytes 786440 | tf_op jit(solution)/shard_map/ppermute | solution.py:451
  57.4 4.4 %collective-permute-done.7 = bf16[64,2048]{1,0:T(8,128)(2,1)S(1)} collective-permute-done((bf16[64,2048]{1,0:T(8,128)(2,1)S(1)}, bf16[64,2048]{1,0:T(8,128)(2,1)S(1)}, u32[]{:S(2)}, u32[]{:S(2)}) %collective-permute-start.7) | collective-permute-done | bytes 262176 | tf_op jit(solution)/shard_map/ppermute | solution.py:451
  61.9 2.1 %collective-permute-start.8 = (bf16[32,2048]{1,0:T(8,128)(2,1)S(1)}, bf16[32,2048]{1,0:T(8,128)(2,1)S(1)}, u32[]{:S(2)}, u32[]{:S(2)}) collective-permute-start(bf16[32,2048]{1,0:T(8,128)(2,1)S(1)} %slice.57), channel_id=1, source_target_pairs={{0,2},{1,5},{2,0},{3,7},{4,6},{5,1},{6,4},{7,3},{8,10},{9,13},{10,... | collective-permute-start | bytes 393224 | tf_op jit(solution)/shard_map/ppermute | solution.py:451
  63.9 3.0 %collective-permute-done.8 = bf16[32,2048]{1,0:T(8,128)(2,1)S(1)} collective-permute-done((bf16[32,2048]{1,0:T(8,128)(2,1)S(1)}, bf16[32,2048]{1,0:T(8,128)(2,1)S(1)}, u32[]{:S(2)}, u32[]{:S(2)}) %collective-permute-start.8) | collective-permute-done | bytes 131104 | tf_op jit(solution)/shard_map/ppermute | solution.py:451
  67.0 2.3 %collective-permute-start.9 = (bf16[16,2048]{1,0:T(8,128)(2,1)S(1)}, bf16[16,2048]{1,0:T(8,128)(2,1)S(1)}, u32[]{:S(2)}, u32[]{:S(2)}) collective-permute-start(bf16[16,2048]{1,0:T(8,128)(2,1)S(1)} %slice.58), channel_id=1, source_target_pairs={{0,16},{1,9},{2,18},{3,11},{4,20},{5,13},{6,22},{7,15},{8,24},{9,1... | collective-permute-start | bytes 196616 | tf_op jit(solution)/shard_map/ppermute | solution.py:451
  69.3 2.9 %collective-permute-done.9 = bf16[16,2048]{1,0:T(8,128)(2,1)S(1)} collective-permute-done((bf16[16,2048]{1,0:T(8,128)(2,1)S(1)}, bf16[16,2048]{1,0:T(8,128)(2,1)S(1)}, u32[]{:S(2)}, u32[]{:S(2)}) %collective-permute-start.9) | collective-permute-done | bytes 65568 | tf_op jit(solution)/shard_map/ppermute | solution.py:451
  72.2 2.2 %collective-permute-start.10 = (bf16[8,2048]{1,0:T(8,128)(2,1)S(1)}, bf16[8,2048]{1,0:T(8,128)(2,1)S(1)}, u32[]{:S(2)}, u32[]{:S(2)}) collective-permute-start(bf16[8,2048]{1,0:T(8,128)(2,1)S(1)} %slice.59), channel_id=1, source_target_pairs={{0,8},{1,17},{2,10},{3,19},{4,12},{5,21},{6,14},{7,23},{8,0},{9,25... | collective-permute-start | bytes 98312 | tf_op jit(solution)/shard_map/ppermute | solution.py:451
  74.4 1.9 %collective-permute-done.10 = bf16[8,2048]{1,0:T(8,128)(2,1)S(1)} collective-permute-done((bf16[8,2048]{1,0:T(8,128)(2,1)S(1)}, bf16[8,2048]{1,0:T(8,128)(2,1)S(1)}, u32[]{:S(2)}, u32[]{:S(2)}) %collective-permute-start.10) | collective-permute-done | bytes 32800 | tf_op jit(solution)/shard_map/ppermute | solution.py:451
  76.3 0.6 fusion.1
  (32 shorter events, 1.5 us)
Async XLA Ops:
  0.6 11.8 %copy-start.4 = (bf16[8,2]{0,1:T(2,128)(2,1)S(1)}, bf16[8,2]{0,1:T(2,128)(2,1)}, u32[]{:S(2)}) copy-start(bf16[8,2]{0,1:T(2,128)(2,1)} %param.39) | copy-start | bytes 100
  0.6 11.9 %copy-start.3 = (s32[8,2]{0,1:T(2,128)S(1)}, s32[8,2]{0,1:T(2,128)}, u32[]{:S(2)}) copy-start(s32[8,2]{0,1:T(2,128)} %param.38) | copy-start | bytes 196
  0.7 11.9 %copy-start.2 = (bf16[2048]{0:T(1024)(128)(2,1)S(1)}, bf16[2048]{0:T(1024)(128)(2,1)}, u32[]{:S(2)}) copy-start(bf16[2048]{0:T(1024)(128)(2,1)} %param.37) | copy-start | bytes 12292
  0.7 12.6 %copy-start = (bf16[16,2048]{1,0:T(8,128)(2,1)S(1)}, bf16[16,2048]{1,0:T(8,128)(2,1)}, u32[]{:S(2)}) copy-start(bf16[16,2048]{1,0:T(8,128)(2,1)} %tokens_ref.1) | copy-start | bytes 196612
  0.7 12.6 %copy-start.1 = (f32[2048]{0:T(1024)S(1)}, f32[2048]{0:T(1024)}, u32[]{:S(2)}) copy-start(f32[2048]{0:T(1024)} %param.30) | copy-start | bytes 24580
  11.8 1.4 %collective-permute-start = (bf16[8,2048]{1,0:T(8,128)(2,1)S(1)}, bf16[8,2048]{1,0:T(8,128)(2,1)S(1)}, u32[]{:S(2)}, u32[]{:S(2)}) collective-permute-start(bf16[8,2048]{1,0:T(8,128)(2,1)S(1)} %get-tuple-element.16), channel_id=1, source_target_pairs={{0,1},{1,0},{2,3},{3,2},{4,5},{5,4},{6,7},{7,6},{8,9},{9,8},{10,11... | collective-permute-start | bytes 98312 | tf_op jit(solution)/shard_map/ppermute | solution.py:455
  13.5 4.9 %collective-permute-start.1 = (bf16[8,2176]{1,0:T(8,128)(2,1)S(1)}, bf16[8,2176]{1,0:T(8,128)(2,1)S(1)}, u32[]{:S(2)}, u32[]{:S(2)}) collective-permute-start(bf16[8,2176]{1,0:T(8,128)(2,1)S(1)} %get-tuple-element.18), channel_id=1, source_target_pairs={{0,8},{1,17},{2,10},{3,19},{4,12},{5,21},{6,14},{7,23},{8,0},{9,25... | collective-permute-start | bytes 104456 | tf_op jit(solution)/shard_map/ppermute | solution.py:451
  18.4 5.3 %collective-permute-start.2 = (bf16[16,2176]{1,0:T(8,128)(2,1)S(1)}, bf16[16,2176]{1,0:T(8,128)(2,1)S(1)}, u32[]{:S(2)}, u32[]{:S(2)}) collective-permute-start(bf16[16,2176]{1,0:T(8,128)(2,1)S(1)} %pad_maximum_fusion), channel_id=1, source_target_pairs={{0,16},{1,9},{2,18},{3,11},{4,20},{5,13},{6,22},{7,15},{8,24},{9,1... | collective-permute-start | bytes 208904 | tf_op jit(solution)/shard_map/ppermute | solution.py:451
  23.7 5.8 %collective-permute-start.3 = (bf16[32,2176]{1,0:T(8,128)(2,1)S(1)}, bf16[32,2176]{1,0:T(8,128)(2,1)S(1)}, u32[]{:S(2)}, u32[]{:S(2)}) collective-permute-start(bf16[32,2176]{1,0:T(8,128)(2,1)S(1)} %get-tuple-element.35.after_hbm), channel_id=1, source_target_pairs={{0,2},{1,5},{2,0},{3,7},{4,6},{5,1},{6,4},{7,3},{8,10},{9,13},{10,... | collective-permute-start | bytes 417800 | tf_op jit(solution)/shard_map/ppermute | solution.py:451
  29.6 7.0 %collective-permute-start.4 = (bf16[64,2176]{1,0:T(8,128)(2,1)S(1)}, bf16[64,2176]{1,0:T(8,128)(2,1)S(1)}, u32[]{:S(2)}, u32[]{:S(2)}) collective-permute-start(bf16[64,2176]{1,0:T(8,128)(2,1)S(1)} %get-tuple-element.31.after_hbm), channel_id=1, source_target_pairs={{0,4},{1,3},{2,6},{3,1},{4,0},{5,7},{6,2},{7,5},{8,12},{9,11},{10,... | collective-permute-start | bytes 835592 | tf_op jit(solution)/shard_map/ppermute | solution.py:451
  36.6 9.6 %collective-permute-start.5 = (bf16[128,2176]{1,0:T(8,128)(2,1)S(1)}, bf16[128,2176]{1,0:T(8,128)(2,1)S(1)}, u32[]{:S(2)}, u32[]{:S(2)}) collective-permute-start(bf16[128,2176]{1,0:T(8,128)(2,1)S(1)} %get-tuple-element.27), channel_id=1, source_target_pairs={{0,1},{1,0},{2,3},{3,2},{4,5},{5,4},{6,7},{7,6},{8,9},{9,8},{10,11... | collective-permute-start | bytes 1671176 | tf_op jit(solution)/shard_map/ppermute | solution.py:455
  53.1 2.1 %collective-permute-start.6 = (bf16[128,2048]{1,0:T(8,128)(2,1)S(1)}, bf16[128,2048]{1,0:T(8,128)(2,1)S(1)}, u32[]{:S(2)}, u32[]{:S(2)}) collective-permute-start(bf16[128,2048]{1,0:T(8,128)(2,1)S(1)} %get-tuple-element.24), channel_id=1, source_target_pairs={{0,1},{1,0},{2,3},{3,2},{4,5},{5,4},{6,7},{7,6},{8,9},{9,8},{10,11... | collective-permute-start | bytes 1572872 | tf_op jit(solution)/shard_map/ppermute | solution.py:455
  55.3 6.4 %collective-permute-start.7 = (bf16[64,2048]{1,0:T(8,128)(2,1)S(1)}, bf16[64,2048]{1,0:T(8,128)(2,1)S(1)}, u32[]{:S(2)}, u32[]{:S(2)}) collective-permute-start(bf16[64,2048]{1,0:T(8,128)(2,1)S(1)} %slice.56), channel_id=1, source_target_pairs={{0,4},{1,3},{2,6},{3,1},{4,0},{5,7},{6,2},{7,5},{8,12},{9,11},{10,... | collective-permute-start | bytes 786440 | tf_op jit(solution)/shard_map/ppermute | solution.py:451
  61.9 5.0 %collective-permute-start.8 = (bf16[32,2048]{1,0:T(8,128)(2,1)S(1)}, bf16[32,2048]{1,0:T(8,128)(2,1)S(1)}, u32[]{:S(2)}, u32[]{:S(2)}) collective-permute-start(bf16[32,2048]{1,0:T(8,128)(2,1)S(1)} %slice.57), channel_id=1, source_target_pairs={{0,2},{1,5},{2,0},{3,7},{4,6},{5,1},{6,4},{7,3},{8,10},{9,13},{10,... | collective-permute-start | bytes 393224 | tf_op jit(solution)/shard_map/ppermute | solution.py:451
  67.0 5.2 %collective-permute-start.9 = (bf16[16,2048]{1,0:T(8,128)(2,1)S(1)}, bf16[16,2048]{1,0:T(8,128)(2,1)S(1)}, u32[]{:S(2)}, u32[]{:S(2)}) collective-permute-start(bf16[16,2048]{1,0:T(8,128)(2,1)S(1)} %slice.58), channel_id=1, source_target_pairs={{0,16},{1,9},{2,18},{3,11},{4,20},{5,13},{6,22},{7,15},{8,24},{9,1... | collective-permute-start | bytes 196616 | tf_op jit(solution)/shard_map/ppermute | solution.py:451
  72.2 4.1 %collective-permute-start.10 = (bf16[8,2048]{1,0:T(8,128)(2,1)S(1)}, bf16[8,2048]{1,0:T(8,128)(2,1)S(1)}, u32[]{:S(2)}, u32[]{:S(2)}) collective-permute-start(bf16[8,2048]{1,0:T(8,128)(2,1)S(1)} %slice.59), channel_id=1, source_target_pairs={{0,8},{1,17},{2,10},{3,19},{4,12},{5,21},{6,14},{7,23},{8,0},{9,25... | collective-permute-start | bytes 98312 | tf_op jit(solution)/shard_map/ppermute | solution.py:451
where the time goes:
time: 77.1 us; the launch traced here: 76.9 us
  Pallas kernels  27.7 us (36%)
  waiting for transfers between devices  26.5 us (34%)
  starting transfers between devices  20.6 us (27%)
  other arithmetic  0.84 us (1%)
  between operations  0.82 us (1%)
    ppermute x8, waiting for transfers between devices, exchange(): return lax.ppermute(array, ('ep', 'tp'), pairs)  24.3 us
    ppermute x8, starting transfers between devices, exchange(): return lax.ppermute(array, ('ep', 'tp'), pairs)  19.4 us
    pallas_call x1, Pallas kernels, attention(): pl.pallas_call(functools.partial(attention_kernel, row_count, group), out...  11.1 us
    pallas_call x2, Pallas kernels, fetch_call(): pl.pallas_call(kernel, out_shape=tuple((pltpu.VMEM(shape, BF16) for shape...  9.52 us
    pallas_call x1, Pallas kernels, feed_forward(): pl.pallas_call(functools.partial(ffn_kernel, members, 512 if width % 512...  6.8 us
    ppermute x3, waiting for transfers between devices, swap(): return lax.ppermute(array, 'tp', [(i, i ^ 1) for i in range(n_tp)])  2.2 us
  transfers between devices with their start and end apart: 11, of which 10 were waited for; matrix products, arithmetic and copies ran while one was open for 0% of the time, Pallas kernels for 12%

commit v1 on v0

--- a/solution.py
+++ b/solution.py
@@ -11,8 +11,11 @@
 HEAD_DIM = 64
 EXPERTS = 8
 LANES = 128
+BLOCK = 256
 EPSILON = 1e-06
 FETCH_FLOPS = 200
+IN_FLIGHT = 8
+GROUP = 8
 F32 = jnp.float32
 BF16 = jnp.bfloat16
 
@@ -38,73 +41,67 @@
 
 
 def attention_kernel(
-    row_count, group,
+    row_count, group, q_parts, o_parts,
     lengths_hbm, tokens_hbm, gain_hbm, bias_hbm,
     wq_hbm, wk_hbm, wv_hbm, wo_hbm, keys_hbm, values_hbm,
     keep_ref, send_ref, new_keys_ref, new_values_ref,
     lengths_ref, tokens_ref, gain_ref, bias_ref,
     wq, wk, wv, wo, keys, values, queries, mixed, later, partial,
-    sem_small, sem_q, sem_kv, sem_k, sem_v, sem_o,
+    sems,
 ):
     seqs, width = tokens_ref.shape
     cache = keys.shape[1]
     q_width = wq.shape[1]
     heads = q_width // HEAD_DIM
     pairs = heads // 2
-    q_parts = sem_q.shape[0]
-    o_parts = sem_o.shape[0]
     groups = seqs // group
     q_rows = width // q_parts
     o_rows = q_width // o_parts
     half = 2 * LANES
 
-    def q_copy(i):
-        rows = pl.ds(i * q_rows, q_rows)
-        return pltpu.make_async_copy(wq_hbm.at[rows], wq.at[rows], sem_q.at[i])
-
-    def o_copy(i):
-        rows = pl.ds(i * o_rows, o_rows)
-        return pltpu.make_async_copy(wo_hbm.at[rows], wo.at[rows], sem_o.at[i])
-
-    def k_copy(i):
-        rows = pl.ds(i * group, group)
-        return pltpu.make_async_copy(keys_hbm.at[rows], keys.at[rows], sem_k.at[i])
-
-    def v_copy(i):
-        rows = pl.ds(i * group, group)
-        return pltpu.make_async_copy(values_hbm.at[rows], values.at[rows], sem_v.at[i])
-
-    small = [
-        pltpu.make_async_copy(source, target, sem_small.at[i])
-        for i, (source, target) in enumerate((
-            (tokens_hbm, tokens_ref), (gain_hbm, gain_ref),
-            (lengths_hbm, lengths_ref), (bias_hbm, bias_ref),
-        ))
+    plan = [
+        (tokens_hbm, tokens_ref), (gain_hbm, gain_ref), (lengths_hbm, lengths_ref),
+        (bias_hbm, bias_ref),
     ]
-    for copy in small:
+    small = len(plan)
+    for i in range(q_parts):
+        part = pl.ds(i * q_rows, q_rows)
+        plan.append((wq_hbm.at[part], wq.at[part]))
+    parts = [pl.ds(i * group, group) for i in range(groups)]
+    plan.append((keys_hbm.at[parts[0]], keys.at[parts[0]]))
+    for i in range(groups):
+        for part in parts[i + 1:i + 2]:
+            plan.append((keys_hbm.at[part], keys.at[part]))
+        plan.append((values_hbm.at[parts[i]], values.at[parts[i]]))
+    plan += [(wk_hbm, wk), (wv_hbm, wv)]
+    for i in range(o_parts):
+        part = pl.ds(i * o_rows, o_rows)
+        plan.append((wo_hbm.at[part], wo.at[part]))
+    copies = [
+        pltpu.make_async_copy(source, target, sems.at[i])
+        for i, (source, target) in enumerate(plan)
+    ]
+    waited = [0]
+    for copy in copies[:small + IN_FLIGHT]:
         copy.start()
-    copy_wk = pltpu.make_async_copy(wk_hbm, wk, sem_kv.at[0])
-    copy_wv = pltpu.make_async_copy(wv_hbm, wv, sem_kv.at[1])
-    for i in range(q_parts):
-        q_copy(i).start()
-    for i in range(groups):
-        k_copy(i).start()
-        v_copy(i).start()
-    copy_wk.start()
-    copy_wv.start()
-    for i in range(o_parts):
-        o_copy(i).start()
+
+    def arrive(count):
+        for _ in range(count):
+            copies[waited[0]].wait()
+            waited[0] += 1
+            following = waited[0] + IN_FLIGHT - 1
+            if waited[0] > small and following < len(copies):
+                copies[following].start()
 
     later_rows = lax.broadcasted_iota(jnp.int32, (2 * half, half), 0) % half
     later_cols = lax.broadcasted_iota(jnp.int32, (2 * half, half), 1)
     later[...] = (later_rows > later_cols).astype(F32).astype(BF16)
 
-    for copy in small:
-        copy.wait()
+    arrive(small)
     normed = normed_block(tokens_ref[...].astype(F32), gain_ref[...])
     query = jnp.zeros((seqs, q_width), F32)
     for i in range(q_parts):
-        q_copy(i).wait()
+        arrive(1)
         query += jnp.dot(
             normed[:, i * q_rows:(i + 1) * q_rows],
             wq[i * q_rows:(i + 1) * q_rows, :],
@@ -134,22 +131,22 @@
     place = lax.broadcasted_iota(jnp.int32, (rows, half), 1)
     blocks = cache // half
 
-    def attend(step, carry):
-        k_copy(step).wait()
-        first = step * group
+    def score(step):
+        arrive(1)
         scores = []
-        for s in range(group):
-            q_seq = queries[pl.ds(pl.multiple_of((first + s) * heads, heads), heads), :]
+        for s in range(step * group, (step + 1) * group):
+            q_seq = queries[pl.ds(s * heads, heads), :].astype(BF16)
             scores.append(
                 lax.dot_general(
-                    q_seq.astype(BF16), keys[first + s], (((1,), (1,)), ((), ())),
-                    preferred_element_type=F32,
+                    q_seq, keys[s], (((1,), (1,)), ((), ())), preferred_element_type=F32
                 )
             )
-        scores = jnp.concatenate(scores, axis=0)
+        return jnp.concatenate(scores, axis=0)
+
+    def weigh(step, scores):
         length = jnp.zeros((rows, 1), jnp.int32)
         for s in range(group):
-            length = jnp.where(seq_of == s, lengths_ref[first + s], length)
+            length = jnp.where(seq_of == s, lengths_ref[step * group + s], length)
         opened, pieces, heads_first = [], [], []
         for n in range(blocks):
             z = scores[:, n * half:(n + 1) * half] * HEAD_DIM ** (-0.5) + bias
@@ -170,19 +167,24 @@
             within = after[n * rows:(n + 1) * rows]
             weights[n] = jnp.exp(opened[n] + within + beyond).astype(BF16)
             beyond = beyond + within[:, 0:1] + heads_first[n]
-        weights = jnp.concatenate(weights, axis=1)
-        v_copy(step).wait()
+        return jnp.concatenate(weights, axis=1)
+
+    def mix(step, weights):
+        arrive(1)
         for s in range(group):
-            mixed[pl.ds(pl.multiple_of((first + s) * heads, heads), heads), :] = jnp.dot(
-                weights[s * heads:(s + 1) * heads], values[first + s],
-                preferred_element_type=F32,
+            seq = step * group + s
+            mixed[pl.ds(seq * heads, heads), :] = jnp.dot(
+                weights[s * heads:(s + 1) * heads], values[seq], preferred_element_type=F32
             )
-        return carry
-
-    lax.fori_loop(0, groups, attend, 0)
-
-    copy_wk.wait()
-    copy_wv.wait()
+
+    scores = score(0)
+    for step in range(groups):
+        following = score(step + 1) if step + 1 < groups else None
+        weights = weigh(step, scores)
+        mix(step, weights)
+        scores = following
+
+    arrive(2)
     new_keys_ref[...] = jnp.dot(normed, wk[...], preferred_element_type=F32).astype(BF16)
     new_values_ref[...] = jnp.dot(normed, wv[...], preferred_element_type=F32).astype(BF16)
 
@@ -198,7 +200,7 @@
     heads_out = jnp.concatenate(joined, axis=1)
     total = jnp.zeros((seqs, width), F32)
     for i in range(o_parts):
-        o_copy(i).wait()
+        arrive(1)
         total += jnp.dot(
             heads_out[:, i * o_rows:(i + 1) * o_rows],
             wo[i * o_rows:(i + 1) * o_rows, :],
@@ -217,14 +219,14 @@
     q_width = w_query.shape[1]
     kv_width = w_key.shape[1]
     heads = q_width // HEAD_DIM
-    group = 4 if seqs % 4 == 0 else 1
+    group = GROUP if seqs % GROUP == 0 else 1
     q_parts = split_of(width, 4)
     o_parts = split_of(q_width, 4)
     dma = pltpu.SemaphoreType.DMA
     half = jax.ShapeDtypeStruct((row_count, width), BF16)
     kv = jax.ShapeDtypeStruct((seqs, kv_width), BF16)
     return pl.pallas_call(
-        functools.partial(attention_kernel, row_count, group),
+        functools.partial(attention_kernel, row_count, group, q_parts, o_parts),
         out_shape=(half, half, kv, kv),
         in_specs=[HBM] * 10,
         out_specs=(VMEM,) * 4,
@@ -243,8 +245,7 @@
             pltpu.VMEM((seqs * heads, LANES), F32),
             pltpu.VMEM((4 * LANES, 2 * LANES), BF16),
             pltpu.VMEM((seqs, width), F32),
-            dma((4,)), dma((q_parts,)), dma((2,)), dma((seqs // group,)), dma((seqs // group,)),
-            dma((o_parts,)),
+            dma((6 + q_parts + o_parts + 2 * (seqs // group),)),
         ],
         compiler_params=pltpu.CompilerParams(vmem_limit_bytes=36 * 2**20),
         name="attention",
@@ -297,10 +298,11 @@
     return pl.ds(pl.multiple_of(lax.axis_index("tp") * units, 8), units)
 
 
-def fetch_all(copies, sems):
+def fetch_kernel(plan, count, *refs):
+    sems = refs[-1]
     copies = [
         pltpu.make_async_copy(source, target, sems.at[i])
-        for i, (source, target) in enumerate(copies)
+        for i, (source, target) in enumerate(plan(refs[1:1 + count], refs[1 + count:-1]))
     ]
     for copy in copies:
         copy.start()
@@ -308,41 +310,10 @@
         copy.wait()
 
 
-def fetch_up_kernel(after_hbm, gate_hbm, up_hbm, dense_gate_hbm, dense_up_hbm, wide, dense, sems):
-    hidden, _, block = wide.shape
-    part = units_part(dense.shape[1])
-    copies = []
-    if block == gate_hbm.shape[1]:
-        copies += [(gate_hbm, wide.at[0]), (up_hbm, wide.at[1])]
-    else:
-        block //= 2
-        for i in range(hidden):
-            cols = pl.ds(i * block, block)
-            copies.append((gate_hbm.at[:, cols], wide.at[i, :, pl.ds(0, block)]))
-            copies.append((up_hbm.at[:, cols], wide.at[i, :, pl.ds(block, block)]))
-    copies.append((dense_gate_hbm.at[part], dense.at[0]))
-    copies.append((dense_up_hbm.at[part], dense.at[1]))
-    fetch_all(copies, sems)
-
-
-def fetch_down_kernel(after_hbm, down_hbm, dense_down_hbm, down, dense, sems):
-    pieces = sems.shape[0] // 2
-    rows = down.shape[0] // pieces
-    dense_rows = dense.shape[0] // pieces
-    first = units_part(dense.shape[0]).start
-    copies = []
-    for i in range(pieces):
-        part = pl.ds(i * rows, rows)
-        copies.append((down_hbm.at[part], down.at[part]))
-        source = pl.ds(pl.multiple_of(first + i * dense_rows, 8), dense_rows)
-        copies.append((dense_down_hbm.at[source], dense.at[pl.ds(i * dense_rows, dense_rows)]))
-    fetch_all(copies, sems)
-
-
-def fetch_call(kernel, after, arrays, shapes, copies):
+def fetch(after, arrays, shapes, copies, plan):
     size = sum(2 * math.prod(shape) for shape in shapes)
     return pl.pallas_call(
-        kernel,
+        functools.partial(fetch_kernel, plan, len(arrays)),
         out_shape=tuple(pltpu.VMEM(shape, BF16) for shape in shapes),
         in_specs=[HBM] * (1 + len(arrays)),
         out_specs=(VMEM,) * len(shapes),
@@ -354,30 +325,68 @@
     )(after, *in_hbm(*arrays))
 
 
-def fetch_weights(after_first, after_second, expert_gate, expert_up, expert_down, dense_gate_w,
-                  dense_up_w, dense_down_w):
+def wide_plan(first, count, gate_hbm, up_hbm, target):
+    pairs = []
+    for i in range(count):
+        cols = pl.ds((first + i) * BLOCK, BLOCK)
+        pairs.append((gate_hbm.at[:, cols], target.at[i, :, pl.ds(0, BLOCK)]))
+        pairs.append((up_hbm.at[:, cols], target.at[i, :, pl.ds(BLOCK, BLOCK)]))
+    return pairs
+
+
+def fetch_weights(after, expert_gate, expert_up, expert_down, dense_gate_w, dense_up_w,
+                  dense_down_w):
     width, units = expert_gate.shape
-    wide = (units // 256, width, 512) if units % 512 == 256 else (2, width, units)
+    blocks = units // BLOCK
+    early = 1
+    joined = units % BLOCK == 0 and blocks > early
     dense_units = dense_gate_w.shape[1] // lax.axis_size("tp")
-    pieces = 4 if units % 64 == 0 and dense_units % 32 == 0 else 1
-    down, dense_down = fetch_call(
-        fetch_down_kernel, after_first, (expert_down, dense_down_w),
-        ((units, width), (dense_units, width)), 2 * pieces,
-    )
-    wide, dense = fetch_call(
-        fetch_up_kernel, after_second,
-        (expert_gate, expert_up, dense_gate_w.T, dense_up_w.T),
-        (wide, (2, dense_units, width)), 2 * max(wide[0], 1) + 2,
-    )
-    return wide, dense, down, dense_down
-
-
-def ffn_kernel(members, out_block, rows_ref, wide, dense, down, dense_down, own_ref, other_ref,
-               hidden_ref):
+
+    def first_plan(sources, targets):
+        part = units_part(dense_units)
+        pairs = [
+            (sources[i].at[part], target)
+            for i, target in enumerate((targets[0].at[0], targets[0].at[1], targets[1]))
+        ]
+        if joined:
+            return pairs + wide_plan(0, early, sources[3], sources[4], targets[2])
+        return pairs + [(sources[3], targets[2].at[0])]
+
+    def second_plan(sources, targets):
+        half = units // 2
+        return [
+            (sources[0].at[pl.ds(i * half, half)], targets[0].at[pl.ds(i * half, half)])
+            for i in range(2)
+        ]
+
+    def third_plan(sources, targets):
+        if joined:
+            return wide_plan(early, blocks - early, *sources, targets[0])
+        return [(sources[1], targets[0].at[0])]
+
+    dense, dense_down, first_wide = fetch(
+        after[0],
+        (dense_gate_w.T, dense_up_w.T, dense_down_w, expert_gate, expert_up),
+        (
+            (2, dense_units, width), (dense_units, width),
+            (early, width, 2 * BLOCK) if joined else (1, width, units),
+        ),
+        3 + (2 * early if joined else 1), first_plan,
+    )
+    down, = fetch(after[1], (expert_down,), ((units, width),), 2, second_plan)
+    last_wide, = fetch(
+        after[2], (expert_gate, expert_up),
+        ((blocks - early, width, 2 * BLOCK) if joined else (1, width, units),),
+        2 * (blocks - early) if joined else 1, third_plan,
+    )
+    return first_wide, last_wide, dense, down, dense_down
+
+
+def ffn_kernel(members, out_block, rows_ref, first_wide, last_wide, dense, down, dense_down,
+               own_ref, other_ref, hidden_ref):
     count, padded = rows_ref.shape
     width = padded - LANES
     units = down.shape[0]
-    hidden, _, block = wide.shape
     device = lax.axis_index("ep") * lax.axis_size("tp") + lax.axis_index("tp")
     expert = device // members
     extra = rows_ref[:, width:].astype(F32)
@@ -390,15 +399,17 @@
         return (gate / (1.0 + jnp.exp(-gate)) * up * scale).astype(BF16)
 
     rows = rows_ref[:, :width]
-    if block == units:
-        gate, up = (jnp.dot(rows, wide[i], preferred_element_type=F32) for i in range(2))
+    if first_wide.shape[2] == units:
+        gate = jnp.dot(rows, first_wide[0], preferred_element_type=F32)
+        up = jnp.dot(rows, last_wide[0], preferred_element_type=F32)
         hidden_ref[...] = activate(gate, up, share)
     else:
-        block //= 2
-        for i in range(hidden):
-            both = jnp.dot(rows, wide[i], preferred_element_type=F32)
-            hidden_ref[:, i * block:(i + 1) * block] = activate(
-                both[:, :block], both[:, block:], share
+        early = first_wide.shape[0]
+        for i in range(units // BLOCK):
+            weights = first_wide[i] if i < early else last_wide[i - early]
+            both = jnp.dot(rows, weights, preferred_element_type=F32)
+            hidden_ref[:, i * BLOCK:(i + 1) * BLOCK] = activate(
+                both[:, :BLOCK], both[:, BLOCK:], share
             )
     dims = (((1,), (1,)), ((), ()))
     gate, up = (
@@ -416,14 +427,14 @@
 def feed_forward(rows, weights, members):
     count, padded = rows.shape
     width = padded - LANES
-    units = weights[2].shape[0]
+    units = weights[3].shape[0]
     return pl.pallas_call(
         functools.partial(ffn_kernel, members, 512 if width % 512 == 0 else width),
         out_shape=(
             jax.ShapeDtypeStruct((count // 2, width), F32),
             jax.ShapeDtypeStruct((count // 2, width), BF16),
         ),
-        in_specs=[VMEM] * 5,
+        in_specs=[VMEM] * 6,
         out_specs=(VMEM,) * 2,
         scratch_shapes=[pltpu.VMEM((count, units), BF16)],
         cost_estimate=pl.CostEstimate(
@@ -436,11 +447,13 @@
 
 def phases_of(n_ep):
     bits = [1 << b for b in range(n_ep.bit_length() - 1)]
-    phases = []
-    while len(bits) >= 2:
+    doublings = []
+    while len(bits) >= 4:
         high, low = bits.pop(), bits.pop()
-        phases += [(low, high), (high, low)]
-    return phases + [(bit, bit) for bit in bits]
+        doublings += [(high, low), (low, high)]
+    doublings += [(bit, bit) for bit in bits[2:]]
+    direct = [(2, 1), (1, 2), (3, 3)] if len(bits) >= 2 else [(bit, bit) for bit in bits]
+    return doublings, direct
 
 
 def exchange(array, masks, n_ep, n_tp):
@@ -469,20 +482,32 @@
     rows, middle = make_middle(
         tokens, keep, swap(send, n_tp), norm_ffn, dense_mix, routes, route_weights
     )
-    phases = phases_of(n_ep)
+    doublings, direct = phases_of(n_ep)
     held = []
-    for masks in phases:
+    for masks in doublings:
         held.append(rows)
         got = exchange(rows, masks, n_ep, n_tp)
         rows = jnp.concatenate([rows, got], axis=0)
+    pieces = [rows]
+    for masks in direct:
+        pieces.append(exchange(rows, masks, n_ep, n_tp))
     weights = fetch_weights(
-        held[-2], held[-1], expert_gate, expert_up, expert_down, dense_gate_w, dense_up_w,
-        dense_down_w,
-    )
+        (held[-2], held[-1], rows), expert_gate, expert_up, expert_down, dense_gate_w,
+        dense_up_w, dense_down_w,
+    )
+    rows = jnp.concatenate(pieces, axis=0)
     rows = jnp.concatenate([rows, swap(rows, n_tp)], axis=0)
     own, other = feed_forward(rows, weights, n_ep * n_tp // EXPERTS)
     total = own + swap(other, n_tp).astype(F32)
-    for masks in reversed(phases):
+    part = total.shape[0] // (len(direct) + 1)
+    sent = [
+        exchange(total[(i + 1) * part:(i + 2) * part].astype(BF16), masks, n_ep, n_tp)
+        for i, masks in enumerate(direct)
+    ]
+    total = total[:part]
+    for got in sent:
+        total = total + got.astype(F32)
+    for masks in reversed(doublings):
         half = total.shape[0] // 2
         got = exchange(total[half:].astype(BF16), masks, n_ep, n_tp)
         total = total[:half] + got.astype(F32)

time: 77.1 us -> 69.2 us (0.90)
  waiting for transfers between devices: 26.5 us -> 23 us
  Pallas kernels: 27.7 us -> 25.3 us
  starting transfers between devices: 20.6 us -> 18.6 us
    ppermute x8 -> x10, waiting for transfers between devices: 24.3 us -> 20.7 us  [exchange(): return lax.ppermute(array, ('ep', 'tp'), pairs)]
    pallas_call x3 -> x4, Pallas kernels: 20.7 us -> 18.3 us  [the longest x3 10.5 us: fetch(): pl.pallas_call(functools.partial(fetch_kernel, plan, len(arrays)), out_sh...]
    ppermute x8 -> x10, starting transfers between devices: 19.4 us -> 17.4 us  [exchange(): return lax.ppermute(array, ('ep', 'tp'), pairs)]
  transfers between devices with their start and end apart: 11 -> 13, of which waited for: 10 -> 9; matrix products, arithmetic and copies ran while one was open for 0% -> 0% of each run, Pallas kernels for 12% -> 15%
where the time goes in v1:
time: 69.2 us; the launch traced here: 69 us
  Pallas kernels  25.3 us (37%)
  waiting for transfers between devices  23 us (33%)
  starting transfers between devices  18.6 us (27%)
  other arithmetic  0.85 us (1%)
  between operations  0.83 us (1%)
    ppermute x10, waiting for transfers between devices, exchange(): return lax.ppermute(array, ('ep', 'tp'), pairs)  20.7 us
    ppermute x10, starting transfers between devices, exchange(): return lax.ppermute(array, ('ep', 'tp'), pairs)  17.4 us
    pallas_call x3, Pallas kernels, fetch(): pl.pallas_call(functools.partial(fetch_kernel, plan, len(arrays)), out_sh...  10.5 us
    pallas_call x1, Pallas kernels, attention(): pl.pallas_call(functools.partial(attention_kernel, row_count, group, q_pa...  7.79 us
    pallas_call x1, Pallas kernels, feed_forward(): pl.pallas_call(functools.partial(ffn_kernel, members, 512 if width % 512...  6.79 us
    ppermute x3, waiting for transfers between devices, swap(): return lax.ppermute(array, 'tp', [(i, i ^ 1) for i in range(n_tp)])  2.2 us
  transfers between devices with their start and end apart: 13, of which 9 were waited for; matrix products, arithmetic and copies ran while one was open for 0% of the time, Pallas kernels for 15%

profile of v1, /device:TPU:0, one launch (start us, length us, event | category | flops | bytes accessed | tf_op | source)
XLA Modules:
  0.0 69.0 jit_solution(5383799336929459325)
XLA Ops:
  0.7 7.8 %attention.1 = (bf16[8,2048]{1,0:T(8,128)(2,1)S(1)}, bf16[8,2048]{1,0:T(8,128)(2,1)S(1)}, bf16[16,128]{1,0:T(8,128)(2,1)}, bf16[16,128]{1,0:T(8,128)(2,1)}) custom-call(s32[16]{0:T(128)} %lengths_hbm.1, bf16[16,2048]{1,0:T(8,128)(2,1)} %tokens_ref.1, f32[1,2048]{1,0:T(1,128)} %bitcast.7, f32[16]{0:T(128)} %bias_hbm.1, bf16[2048,1024]{1,0:T(8,128)(2,1)} %wq_hbm.1, ...), custom_call_target="tpu_custom_call" | custom-call | tf_op jit(solution)/shard_map/attention/pallas_call | solution.py:228
  8.5 0.6 collective-permute-start
  9.2 0.7 collective-permute-done.got_ref
  10.1 4.0 %collective-permute-start.1 = (bf16[8,2176]{1,0:T(8,128)(2,1)S(1)}, bf16[8,2176]{1,0:T(8,128)(2,1)S(1)}, u32[]{:S(2)}, u32[]{:S(2)}) collective-permute-start(bf16[8,2176]{1,0:T(8,128)(2,1)S(1)} %get-tuple-element.17.refs_0_), channel_id=1, source_target_pairs={{0,16},{1,9},{2,18},{3,11},{4,20},{5,13},{6,22},{7,15},{8,24},{9,1... | collective-permute-start | bytes 104456 | tf_op jit(solution)/shard_map/ppermute | solution.py:464
  14.1 1.9 %collective-permute-done.1 = bf16[8,2176]{1,0:T(8,128)(2,1)S(1)} collective-permute-done((bf16[8,2176]{1,0:T(8,128)(2,1)S(1)}, bf16[8,2176]{1,0:T(8,128)(2,1)S(1)}, u32[]{:S(2)}, u32[]{:S(2)}) %collective-permute-start.1) | collective-permute-done | bytes 34848 | tf_op jit(solution)/shard_map/ppermute | solution.py:464
  16.1 2.0 %collective-permute-start.2 = (bf16[16,2176]{1,0:T(8,128)(2,1)S(1)}, bf16[16,2176]{1,0:T(8,128)(2,1)S(1)}, u32[]{:S(2)}, u32[]{:S(2)}) collective-permute-start(bf16[16,2176]{1,0:T(8,128)(2,1)S(1)} %get-tuple-element.42.refs_0_), channel_id=1, source_target_pairs={{0,8},{1,17},{2,10},{3,19},{4,12},{5,21},{6,14},{7,23},{8,0},{9,25... | collective-permute-start | bytes 208904 | tf_op jit(solution)/shard_map/ppermute | solution.py:464
  18.0 2.4 %collective-permute-done.2 = bf16[16,2176]{1,0:T(8,128)(2,1)S(1)} collective-permute-done((bf16[16,2176]{1,0:T(8,128)(2,1)S(1)}, bf16[16,2176]{1,0:T(8,128)(2,1)S(1)}, u32[]{:S(2)}, u32[]{:S(2)}) %collective-permute-start.2) | collective-permute-done | bytes 69664 | tf_op jit(solution)/shard_map/ppermute | solution.py:464
  20.5 1.9 %collective-permute-start.3 = (bf16[32,2176]{1,0:T(8,128)(2,1)S(1)}, bf16[32,2176]{1,0:T(8,128)(2,1)S(1)}, u32[]{:S(2)}, u32[]{:S(2)}) collective-permute-start(bf16[32,2176]{1,0:T(8,128)(2,1)S(1)} %get-tuple-element.38.refs_0_), channel_id=1, source_target_pairs={{0,4},{1,3},{2,6},{3,1},{4,0},{5,7},{6,2},{7,5},{8,12},{9,11},{10,... | collective-permute-start | bytes 417800 | tf_op jit(solution)/shard_map/ppermute | solution.py:464
  22.4 1.4 %collective-permute-start.5 = (bf16[32,2176]{1,0:T(8,128)(2,1)S(1)}, bf16[32,2176]{1,0:T(8,128)(2,1)S(1)}, u32[]{:S(2)}, u32[]{:S(2)}) collective-permute-start(bf16[32,2176]{1,0:T(8,128)(2,1)S(1)} %get-tuple-element.38.refs_0_), channel_id=1, source_target_pairs={{0,6},{1,7},{2,4},{3,5},{4,2},{5,3},{6,0},{7,1},{8,14},{9,15},{10,... | collective-permute-start | bytes 417800 | tf_op jit(solution)/shard_map/ppermute | solution.py:464
  24.0 5.7 %collective-permute-done.3 = bf16[32,2176]{1,0:T(8,128)(2,1)S(1)} collective-permute-done((bf16[32,2176]{1,0:T(8,128)(2,1)S(1)}, bf16[32,2176]{1,0:T(8,128)(2,1)S(1)}, u32[]{:S(2)}, u32[]{:S(2)}) %collective-permute-start.3) | collective-permute-done | bytes 139296 | tf_op jit(solution)/shard_map/ppermute | solution.py:464
  29.9 2.4 %shard_map.211 = (bf16[2,224,2048]{2,1,0:T(8,128)(2,1)S(1)}, bf16[224,2048]{1,0:T(8,128)(2,1)S(1)}, bf16[1,2048,512]{2,1,0:T(8,128)(2,1)S(1)}) custom-call(bf16[8,2176]{1,0:T(8,128)(2,1)S(1)} %get-tuple-element.17.refs_0_, bf16[448,2048]{1,0:T(8,128)(2,1)} %bitcast.5, bf16[448,2048]{1,0:T(8,128)(2,1)} %bitcast.6, bf16[448,2048]{1,0:T(8,128)(2,1)} %refs_3_.1, ...), custom_call_target="tpu_custom_call" | custom-call | flops 969932800 | bytes 4849664 | tf_op jit(solution)/shard_map/pallas_call | solution.py:315
  32.3 3.2 %shard_map.213.down = bf16[1792,2048]{1,0:T(8,128)(2,1)S(1)} custom-call(bf16[16,2176]{1,0:T(8,128)(2,1)S(1)} %get-tuple-element.42.refs_0_, bf16[1792,2048]{1,0:T(8,128)(2,1)} %refs_1_.3), custom_call_target="tpu_custom_call" | custom-call | flops 1468006400 | bytes 7340032 | tf_op jit(solution)/shard_map/pallas_call | solution.py:315
  35.5 4.9 %shard_map.212.last_wide = bf16[6,2048,512]{2,1,0:T(8,128)(2,1)S(1)} custom-call(bf16[32,2176]{1,0:T(8,128)(2,1)S(1)} %get-tuple-element.38.refs_0_, bf16[2048,1792]{1,0:T(8,128)(2,1)} %refs_1_.2, bf16[2048,1792]{1,0:T(8,128)(2,1)} %refs_2_.1), custom_call_target="tpu_custom_call" | custom-call | flops 2516582400 | bytes 12582912 | tf_op jit(solution)/shard_map/pallas_call | solution.py:315
  40.5 6.8 %feed_forward.1 = (f32[128,2048]{1,0:T(8,128)S(1)}, bf16[128,2048]{1,0:T(8,128)(2,1)S(1)}) custom-call(bf16[256,2176]{1,0:T(8,128)(2,1)S(1)} %constant_dynamic-update-slice_fusion.11.rows_ref, bf16[1,2048,512]{2,1,0:T(8,128)(2,1)S(1)} %get-tuple-element.18.first_wide, bf16[6,2048,512]{2,1,0:T(8,128)(2,1)S(1)} %shard_map.212.last_wide, ...), custom_call_target="tpu_custom_call" | custom-call | flops 5637144576 | tf_op jit(solution)/shard_map/feed_forward/pallas_call | solution.py:431
  47.3 0.6 collective-permute-start.7
  47.9 1.5 %collective-permute-done.7 = bf16[128,2048]{1,0:T(8,128)(2,1)S(1)} collective-permute-done((bf16[128,2048]{1,0:T(8,128)(2,1)S(1)}, bf16[128,2048]{1,0:T(8,128)(2,1)S(1)}, u32[]{:S(2)}, u32[]{:S(2)}) %collective-permute-start.7) | collective-permute-done | bytes 524320 | tf_op jit(solution)/shard_map/ppermute | solution.py:468
  49.7 0.7 %collective-permute-start.8 = (bf16[32,2048]{1,0:T(8,128)(2,1)S(1)}, bf16[32,2048]{1,0:T(8,128)(2,1)S(1)}, u32[]{:S(2)}, u32[]{:S(2)}) collective-permute-start(bf16[32,2048]{1,0:T(8,128)(2,1)S(1)} %get-tuple-element.27), channel_id=1, source_target_pairs={{0,4},{1,3},{2,6},{3,1},{4,0},{5,7},{6,2},{7,5},{8,12},{9,11},{10,... | collective-permute-start | bytes 393224 | tf_op jit(solution)/shard_map/ppermute | solution.py:464
  50.4 2.3 %collective-permute-start.10 = (bf16[32,2048]{1,0:T(8,128)(2,1)S(1)}, bf16[32,2048]{1,0:T(8,128)(2,1)S(1)}, u32[]{:S(2)}, u32[]{:S(2)}) collective-permute-start(bf16[32,2048]{1,0:T(8,128)(2,1)S(1)} %get-tuple-element.28), channel_id=1, source_target_pairs={{0,6},{1,7},{2,4},{3,5},{4,2},{5,3},{6,0},{7,1},{8,14},{9,15},{10,... | collective-permute-start | bytes 393224 | tf_op jit(solution)/shard_map/ppermute | solution.py:464
  53.2 4.7 %collective-permute-done.8 = bf16[32,2048]{1,0:T(8,128)(2,1)S(1)} collective-permute-done((bf16[32,2048]{1,0:T(8,128)(2,1)S(1)}, bf16[32,2048]{1,0:T(8,128)(2,1)S(1)}, u32[]{:S(2)}, u32[]{:S(2)}) %collective-permute-start.8) | collective-permute-done | bytes 131104 | tf_op jit(solution)/shard_map/ppermute | solution.py:464
  58.4 1.8 %collective-permute-start.11 = (bf16[16,2048]{1,0:T(8,128)(2,1)S(1)}, bf16[16,2048]{1,0:T(8,128)(2,1)S(1)}, u32[]{:S(2)}, u32[]{:S(2)}) collective-permute-start(bf16[16,2048]{1,0:T(8,128)(2,1)S(1)} %slice.58), channel_id=1, source_target_pairs={{0,8},{1,17},{2,10},{3,19},{4,12},{5,21},{6,14},{7,23},{8,0},{9,25... | collective-permute-start | bytes 196616 | tf_op jit(solution)/shard_map/ppermute | solution.py:464
  60.2 3.3 %collective-permute-done.11 = bf16[16,2048]{1,0:T(8,128)(2,1)S(1)} collective-permute-done((bf16[16,2048]{1,0:T(8,128)(2,1)S(1)}, bf16[16,2048]{1,0:T(8,128)(2,1)S(1)}, u32[]{:S(2)}, u32[]{:S(2)}) %collective-permute-start.11) | collective-permute-done | bytes 65568 | tf_op jit(solution)/shard_map/ppermute | solution.py:464
  63.5 2.5 %collective-permute-start.12 = (bf16[8,2048]{1,0:T(8,128)(2,1)S(1)}, bf16[8,2048]{1,0:T(8,128)(2,1)S(1)}, u32[]{:S(2)}, u32[]{:S(2)}) collective-permute-start(bf16[8,2048]{1,0:T(8,128)(2,1)S(1)} %slice.59), channel_id=1, source_target_pairs={{0,16},{1,9},{2,18},{3,11},{4,20},{5,13},{6,22},{7,15},{8,24},{9,1... | collective-permute-start | bytes 98312 | tf_op jit(solution)/shard_map/ppermute | solution.py:464
  66.0 2.4 %collective-permute-done.12 = bf16[8,2048]{1,0:T(8,128)(2,1)S(1)} collective-permute-done((bf16[8,2048]{1,0:T(8,128)(2,1)S(1)}, bf16[8,2048]{1,0:T(8,128)(2,1)S(1)}, u32[]{:S(2)}, u32[]{:S(2)}) %collective-permute-start.12) | collective-permute-done | bytes 32800 | tf_op jit(solution)/shard_map/ppermute | solution.py:464
  68.4 0.6 fusion.3
  (35 shorter events, 2.1 us)
Async XLA Ops:
  0.6 8.4 %copy-start.4 = (bf16[8,2]{0,1:T(2,128)(2,1)S(1)}, bf16[8,2]{0,1:T(2,128)(2,1)}, u32[]{:S(2)}) copy-start(bf16[8,2]{0,1:T(2,128)(2,1)} %param.39) | copy-start | bytes 100
  0.6 8.5 %copy-start.3 = (s32[8,2]{0,1:T(2,128)S(1)}, s32[8,2]{0,1:T(2,128)}, u32[]{:S(2)}) copy-start(s32[8,2]{0,1:T(2,128)} %param.38) | copy-start | bytes 196
  0.7 8.6 %copy-start.2 = (bf16[2048]{0:T(1024)(128)(2,1)S(1)}, bf16[2048]{0:T(1024)(128)(2,1)}, u32[]{:S(2)}) copy-start(bf16[2048]{0:T(1024)(128)(2,1)} %param.37) | copy-start | bytes 12292
  0.7 9.2 %copy-start = (bf16[16,2048]{1,0:T(8,128)(2,1)S(1)}, bf16[16,2048]{1,0:T(8,128)(2,1)}, u32[]{:S(2)}) copy-start(bf16[16,2048]{1,0:T(8,128)(2,1)} %tokens_ref.1) | copy-start | bytes 196612
  0.7 9.2 %copy-start.1 = (f32[2048]{0:T(1024)S(1)}, f32[2048]{0:T(1024)}, u32[]{:S(2)}) copy-start(f32[2048]{0:T(1024)} %param.30) | copy-start | bytes 24580
  8.5 1.4 %collective-permute-start = (bf16[8,2048]{1,0:T(8,128)(2,1)S(1)}, bf16[8,2048]{1,0:T(8,128)(2,1)S(1)}, u32[]{:S(2)}, u32[]{:S(2)}) collective-permute-start(bf16[8,2048]{1,0:T(8,128)(2,1)S(1)} %get-tuple-element.15), channel_id=1, source_target_pairs={{0,1},{1,0},{2,3},{3,2},{4,5},{5,4},{6,7},{7,6},{8,9},{9,8},{10,11... | collective-permute-start | bytes 98312 | tf_op jit(solution)/shard_map/ppermute | solution.py:468
  10.1 5.9 %collective-permute-start.1 = (bf16[8,2176]{1,0:T(8,128)(2,1)S(1)}, bf16[8,2176]{1,0:T(8,128)(2,1)S(1)}, u32[]{:S(2)}, u32[]{:S(2)}) collective-permute-start(bf16[8,2176]{1,0:T(8,128)(2,1)S(1)} %get-tuple-element.17.refs_0_), channel_id=1, source_target_pairs={{0,16},{1,9},{2,18},{3,11},{4,20},{5,13},{6,22},{7,15},{8,24},{9,1... | collective-permute-start | bytes 104456 | tf_op jit(solution)/shard_map/ppermute | solution.py:464
  16.1 4.4 %collective-permute-start.2 = (bf16[16,2176]{1,0:T(8,128)(2,1)S(1)}, bf16[16,2176]{1,0:T(8,128)(2,1)S(1)}, u32[]{:S(2)}, u32[]{:S(2)}) collective-permute-start(bf16[16,2176]{1,0:T(8,128)(2,1)S(1)} %get-tuple-element.42.refs_0_), channel_id=1, source_target_pairs={{0,8},{1,17},{2,10},{3,19},{4,12},{5,21},{6,14},{7,23},{8,0},{9,25... | collective-permute-start | bytes 208904 | tf_op jit(solution)/shard_map/ppermute | solution.py:464
  20.5 9.2 %collective-permute-start.3 = (bf16[32,2176]{1,0:T(8,128)(2,1)S(1)}, bf16[32,2176]{1,0:T(8,128)(2,1)S(1)}, u32[]{:S(2)}, u32[]{:S(2)}) collective-permute-start(bf16[32,2176]{1,0:T(8,128)(2,1)S(1)} %get-tuple-element.38.refs_0_), channel_id=1, source_target_pairs={{0,4},{1,3},{2,6},{3,1},{4,0},{5,7},{6,2},{7,5},{8,12},{9,11},{10,... | collective-permute-start | bytes 417800 | tf_op jit(solution)/shard_map/ppermute | solution.py:464
  22.4 7.4 %collective-permute-start.5 = (bf16[32,2176]{1,0:T(8,128)(2,1)S(1)}, bf16[32,2176]{1,0:T(8,128)(2,1)S(1)}, u32[]{:S(2)}, u32[]{:S(2)}) collective-permute-start(bf16[32,2176]{1,0:T(8,128)(2,1)S(1)} %get-tuple-element.38.refs_0_), channel_id=1, source_target_pairs={{0,6},{1,7},{2,4},{3,5},{4,2},{5,3},{6,0},{7,1},{8,14},{9,15},{10,... | collective-permute-start | bytes 417800 | tf_op jit(solution)/shard_map/ppermute | solution.py:464
  23.8 5.9 %collective-permute-start.4 = (bf16[32,2176]{1,0:T(8,128)(2,1)S(1)}, bf16[32,2176]{1,0:T(8,128)(2,1)S(1)}, u32[]{:S(2)}, u32[]{:S(2)}) collective-permute-start(bf16[32,2176]{1,0:T(8,128)(2,1)S(1)} %get-tuple-element.38.refs_0_), channel_id=1, source_target_pairs={{0,2},{1,5},{2,0},{3,7},{4,6},{5,1},{6,4},{7,3},{8,10},{9,13},{10,... | collective-permute-start | bytes 417800 | tf_op jit(solution)/shard_map/ppermute | solution.py:464
  29.8 10.6 %collective-permute-start.6 = (bf16[128,2176]{1,0:T(8,128)(2,1)S(1)}, bf16[128,2176]{1,0:T(8,128)(2,1)S(1)}, u32[]{:S(2)}, u32[]{:S(2)}) collective-permute-start(bf16[128,2176]{1,0:T(8,128)(2,1)S(1)} %get-tuple-element.30), channel_id=1, source_target_pairs={{0,1},{1,0},{2,3},{3,2},{4,5},{5,4},{6,7},{7,6},{8,9},{9,8},{10,11... | collective-permute-start | bytes 1671176 | tf_op jit(solution)/shard_map/ppermute | solution.py:468
  47.3 2.2 %collective-permute-start.7 = (bf16[128,2048]{1,0:T(8,128)(2,1)S(1)}, bf16[128,2048]{1,0:T(8,128)(2,1)S(1)}, u32[]{:S(2)}, u32[]{:S(2)}) collective-permute-start(bf16[128,2048]{1,0:T(8,128)(2,1)S(1)} %get-tuple-element.22), channel_id=1, source_target_pairs={{0,1},{1,0},{2,3},{3,2},{4,5},{5,4},{6,7},{7,6},{8,9},{9,8},{10,11... | collective-permute-start | bytes 1572872 | tf_op jit(solution)/shard_map/ppermute | solution.py:468
  49.7 8.3 %collective-permute-start.8 = (bf16[32,2048]{1,0:T(8,128)(2,1)S(1)}, bf16[32,2048]{1,0:T(8,128)(2,1)S(1)}, u32[]{:S(2)}, u32[]{:S(2)}) collective-permute-start(bf16[32,2048]{1,0:T(8,128)(2,1)S(1)} %get-tuple-element.27), channel_id=1, source_target_pairs={{0,4},{1,3},{2,6},{3,1},{4,0},{5,7},{6,2},{7,5},{8,12},{9,11},{10,... | collective-permute-start | bytes 393224 | tf_op jit(solution)/shard_map/ppermute | solution.py:464
  50.4 7.5 %collective-permute-start.10 = (bf16[32,2048]{1,0:T(8,128)(2,1)S(1)}, bf16[32,2048]{1,0:T(8,128)(2,1)S(1)}, u32[]{:S(2)}, u32[]{:S(2)}) collective-permute-start(bf16[32,2048]{1,0:T(8,128)(2,1)S(1)} %get-tuple-element.28), channel_id=1, source_target_pairs={{0,6},{1,7},{2,4},{3,5},{4,2},{5,3},{6,0},{7,1},{8,14},{9,15},{10,... | collective-permute-start | bytes 393224 | tf_op jit(solution)/shard_map/ppermute | solution.py:464
  52.7 5.7 %collective-permute-start.9 = (bf16[32,2048]{1,0:T(8,128)(2,1)S(1)}, bf16[32,2048]{1,0:T(8,128)(2,1)S(1)}, u32[]{:S(2)}, u32[]{:S(2)}) collective-permute-start(bf16[32,2048]{1,0:T(8,128)(2,1)S(1)} %get-tuple-element.29), channel_id=1, source_target_pairs={{0,2},{1,5},{2,0},{3,7},{4,6},{5,1},{6,4},{7,3},{8,10},{9,13},{10,... | collective-permute-start | bytes 393224 | tf_op jit(solution)/shard_map/ppermute | solution.py:464
  58.4 5.0 %collective-permute-start.11 = (bf16[16,2048]{1,0:T(8,128)(2,1)S(1)}, bf16[16,2048]{1,0:T(8,128)(2,1)S(1)}, u32[]{:S(2)}, u32[]{:S(2)}) collective-permute-start(bf16[16,2048]{1,0:T(8,128)(2,1)S(1)} %slice.58), channel_id=1, source_target_pairs={{0,8},{1,17},{2,10},{3,19},{4,12},{5,21},{6,14},{7,23},{8,0},{9,25... | collective-permute-start | bytes 196616 | tf_op jit(solution)/shard_map/ppermute | solution.py:464
  63.5 4.9 %collective-permute-start.12 = (bf16[8,2048]{1,0:T(8,128)(2,1)S(1)}, bf16[8,2048]{1,0:T(8,128)(2,1)S(1)}, u32[]{:S(2)}, u32[]{:S(2)}) collective-permute-start(bf16[8,2048]{1,0:T(8,128)(2,1)S(1)} %slice.59), channel_id=1, source_target_pairs={{0,16},{1,9},{2,18},{3,11},{4,20},{5,13},{6,22},{7,15},{8,24},{9,1... | collective-permute-start | bytes 98312 | tf_op jit(solution)/shard_map/ppermute | solution.py:464

commit v2 on v1

--- a/solution.py
+++ b/solution.py
@@ -499,15 +499,24 @@
     rows = jnp.concatenate([rows, swap(rows, n_tp)], axis=0)
     own, other = feed_forward(rows, weights, n_ep * n_tp // EXPERTS)
     total = own + swap(other, n_tp).astype(F32)
-    part = total.shape[0] // (len(direct) + 1)
-    sent = [
-        exchange(total[(i + 1) * part:(i + 2) * part].astype(BF16), masks, n_ep, n_tp)
-        for i, masks in enumerate(direct)
-    ]
-    total = total[:part]
-    for got in sent:
-        total = total + got.astype(F32)
-    for masks in reversed(doublings):
+    part = total.shape[0] // (2 * (len(direct) + 1))
+    sums = []
+    for side in (1, 0):
+        sent = [
+            exchange(
+                total[(2 * i + 2 + side) * part:(2 * i + 3 + side) * part].astype(BF16),
+                masks, n_ep, n_tp,
+            )
+            for i, masks in enumerate(direct)
+        ]
+        summed = total[side * part:(side + 1) * part]
+        for got in sent:
+            summed = summed + got.astype(F32)
+        sums.append(summed)
+    second, total = sums
+    got = exchange(second.astype(BF16), doublings[-1], n_ep, n_tp)
+    total = total + got.astype(F32)
+    for masks in reversed(doublings[:-1]):
         half = total.shape[0] // 2
         got = exchange(total[half:].astype(BF16), masks, n_ep, n_tp)
         total = total[:half] + got.astype(F32)

time: 69.2 us -> 67.2 us (0.971)
  waiting for transfers between devices: 23 us -> 16.8 us
  starting transfers between devices: 18.6 us -> 22.8 us
    ppermute x10 -> x13, waiting for transfers between devices: 20.7 us -> 14.6 us  [exchange(): return lax.ppermute(array, ('ep', 'tp'), pairs)]
    ppermute x10 -> x13, starting transfers between devices: 17.4 us -> 21.5 us  [exchange(): return lax.ppermute(array, ('ep', 'tp'), pairs)]
  transfers between devices with their start and end apart: 13 -> 16, of which waited for: 9 -> 9; matrix products, arithmetic and copies ran while one was open for 0% -> 0% of each run, Pallas kernels for 15% -> 16%
where the time goes in v2:
time: 67.2 us; the launch traced here: 67 us
  Pallas kernels  25.3 us (38%)
  starting transfers between devices  22.8 us (34%)
  waiting for transfers between devices  16.8 us (25%)
  other arithmetic  0.85 us (1%)
  between operations  0.83 us (1%)
    ppermute x13, starting transfers between devices, exchange(): return lax.ppermute(array, ('ep', 'tp'), pairs)  21.5 us
    ppermute x13, waiting for transfers between devices, exchange(): return lax.ppermute(array, ('ep', 'tp'), pairs)  14.6 us
    pallas_call x3, Pallas kernels, fetch(): pl.pallas_call(functools.partial(fetch_kernel, plan, len(arrays)), out_sh...  10.5 us
    pallas_call x1, Pallas kernels, attention(): pl.pallas_call(functools.partial(attention_kernel, row_count, group, q_pa...  7.79 us
    pallas_call x1, Pallas kernels, feed_forward(): pl.pallas_call(functools.partial(ffn_kernel, members, 512 if width % 512...  6.79 us
    ppermute x3, waiting for transfers between devices, swap(): return lax.ppermute(array, 'tp', [(i, i ^ 1) for i in range(n_tp)])  2.2 us
  transfers between devices with their start and end apart: 16, of which 9 were waited for; matrix products, arithmetic and copies ran while one was open for 0% of the time, Pallas kernels for 16%

profile of v2, /device:TPU:0, one launch (start us, length us, event | category | flops | bytes accessed | tf_op | source)
XLA Modules:
  0.0 67.0 jit_solution(7641035552264814424)
XLA Ops:
  0.7 7.8 %attention.1 = (bf16[8,2048]{1,0:T(8,128)(2,1)S(1)}, bf16[8,2048]{1,0:T(8,128)(2,1)S(1)}, bf16[16,128]{1,0:T(8,128)(2,1)}, bf16[16,128]{1,0:T(8,128)(2,1)}) custom-call(s32[16]{0:T(128)} %lengths_hbm.1, bf16[16,2048]{1,0:T(8,128)(2,1)} %tokens_ref.1, f32[1,2048]{1,0:T(1,128)} %bitcast.7, f32[16]{0:T(128)} %bias_hbm.1, bf16[2048,1024]{1,0:T(8,128)(2,1)} %wq_hbm.1, ...), custom_call_target="tpu_custom_call" | custom-call | tf_op jit(solution)/shard_map/attention/pallas_call | solution.py:228
  9.2 0.7 collective-permute-done.got_ref
  10.1 4.0 %collective-permute-start.1 = (bf16[8,2176]{1,0:T(8,128)(2,1)S(1)}, bf16[8,2176]{1,0:T(8,128)(2,1)S(1)}, u32[]{:S(2)}, u32[]{:S(2)}) collective-permute-start(bf16[8,2176]{1,0:T(8,128)(2,1)S(1)} %get-tuple-element.17.refs_0_), channel_id=1, source_target_pairs={{0,16},{1,9},{2,18},{3,11},{4,20},{5,13},{6,22},{7,15},{8,24},{9,1... | collective-permute-start | bytes 104456 | tf_op jit(solution)/shard_map/ppermute | solution.py:464
  14.1 1.9 %collective-permute-done.1 = bf16[8,2176]{1,0:T(8,128)(2,1)S(1)} collective-permute-done((bf16[8,2176]{1,0:T(8,128)(2,1)S(1)}, bf16[8,2176]{1,0:T(8,128)(2,1)S(1)}, u32[]{:S(2)}, u32[]{:S(2)}) %collective-permute-start.1) | collective-permute-done | bytes 34848 | tf_op jit(solution)/shard_map/ppermute | solution.py:464
  16.1 2.0 %collective-permute-start.2 = (bf16[16,2176]{1,0:T(8,128)(2,1)S(1)}, bf16[16,2176]{1,0:T(8,128)(2,1)S(1)}, u32[]{:S(2)}, u32[]{:S(2)}) collective-permute-start(bf16[16,2176]{1,0:T(8,128)(2,1)S(1)} %get-tuple-element.45.refs_0_), channel_id=1, source_target_pairs={{0,8},{1,17},{2,10},{3,19},{4,12},{5,21},{6,14},{7,23},{8,0},{9,25... | collective-permute-start | bytes 208904 | tf_op jit(solution)/shard_map/ppermute | solution.py:464
  18.0 2.4 %collective-permute-done.2 = bf16[16,2176]{1,0:T(8,128)(2,1)S(1)} collective-permute-done((bf16[16,2176]{1,0:T(8,128)(2,1)S(1)}, bf16[16,2176]{1,0:T(8,128)(2,1)S(1)}, u32[]{:S(2)}, u32[]{:S(2)}) %collective-permute-start.2) | collective-permute-done | bytes 69664 | tf_op jit(solution)/shard_map/ppermute | solution.py:464
  20.5 1.9 %collective-permute-start.3 = (bf16[32,2176]{1,0:T(8,128)(2,1)S(1)}, bf16[32,2176]{1,0:T(8,128)(2,1)S(1)}, u32[]{:S(2)}, u32[]{:S(2)}) collective-permute-start(bf16[32,2176]{1,0:T(8,128)(2,1)S(1)} %get-tuple-element.41.refs_0_), channel_id=1, source_target_pairs={{0,4},{1,3},{2,6},{3,1},{4,0},{5,7},{6,2},{7,5},{8,12},{9,11},{10,... | collective-permute-start | bytes 417800 | tf_op jit(solution)/shard_map/ppermute | solution.py:464
  22.4 1.4 %collective-permute-start.5 = (bf16[32,2176]{1,0:T(8,128)(2,1)S(1)}, bf16[32,2176]{1,0:T(8,128)(2,1)S(1)}, u32[]{:S(2)}, u32[]{:S(2)}) collective-permute-start(bf16[32,2176]{1,0:T(8,128)(2,1)S(1)} %get-tuple-element.41.refs_0_), channel_id=1, source_target_pairs={{0,6},{1,7},{2,4},{3,5},{4,2},{5,3},{6,0},{7,1},{8,14},{9,15},{10,... | collective-permute-start | bytes 417800 | tf_op jit(solution)/shard_map/ppermute | solution.py:464
  24.0 5.7 %collective-permute-done.3 = bf16[32,2176]{1,0:T(8,128)(2,1)S(1)} collective-permute-done((bf16[32,2176]{1,0:T(8,128)(2,1)S(1)}, bf16[32,2176]{1,0:T(8,128)(2,1)S(1)}, u32[]{:S(2)}, u32[]{:S(2)}) %collective-permute-start.3) | collective-permute-done | bytes 139296 | tf_op jit(solution)/shard_map/ppermute | solution.py:464
  29.9 2.4 %shard_map.211 = (bf16[2,224,2048]{2,1,0:T(8,128)(2,1)S(1)}, bf16[224,2048]{1,0:T(8,128)(2,1)S(1)}, bf16[1,2048,512]{2,1,0:T(8,128)(2,1)S(1)}) custom-call(bf16[8,2176]{1,0:T(8,128)(2,1)S(1)} %get-tuple-element.17.refs_0_, bf16[448,2048]{1,0:T(8,128)(2,1)} %bitcast.5, bf16[448,2048]{1,0:T(8,128)(2,1)} %bitcast.6, bf16[448,2048]{1,0:T(8,128)(2,1)} %refs_3_.1, ...), custom_call_target="tpu_custom_call" | custom-call | flops 969932800 | bytes 4849664 | tf_op jit(solution)/shard_map/pallas_call | solution.py:315
  32.3 3.2 %shard_map.213.down = bf16[1792,2048]{1,0:T(8,128)(2,1)S(1)} custom-call(bf16[16,2176]{1,0:T(8,128)(2,1)S(1)} %get-tuple-element.45.refs_0_, bf16[1792,2048]{1,0:T(8,128)(2,1)} %refs_1_.3), custom_call_target="tpu_custom_call" | custom-call | flops 1468006400 | bytes 7340032 | tf_op jit(solution)/shard_map/pallas_call | solution.py:315
  35.5 4.9 %shard_map.212.last_wide = bf16[6,2048,512]{2,1,0:T(8,128)(2,1)S(1)} custom-call(bf16[32,2176]{1,0:T(8,128)(2,1)S(1)} %get-tuple-element.41.refs_0_, bf16[2048,1792]{1,0:T(8,128)(2,1)} %refs_1_.2, bf16[2048,1792]{1,0:T(8,128)(2,1)} %refs_2_.1), custom_call_target="tpu_custom_call" | custom-call | flops 2516582400 | bytes 12582912 | tf_op jit(solution)/shard_map/pallas_call | solution.py:315
  40.5 6.8 %feed_forward.1 = (f32[128,2048]{1,0:T(8,128)S(1)}, bf16[128,2048]{1,0:T(8,128)(2,1)S(1)}) custom-call(bf16[256,2176]{1,0:T(8,128)(2,1)S(1)} %constant_dynamic-update-slice_fusion.11.rows_ref, bf16[1,2048,512]{2,1,0:T(8,128)(2,1)S(1)} %get-tuple-element.18.first_wide, bf16[6,2048,512]{2,1,0:T(8,128)(2,1)S(1)} %shard_map.212.last_wide, ...), custom_call_target="tpu_custom_call" | custom-call | flops 5637144576 | tf_op jit(solution)/shard_map/feed_forward/pallas_call | solution.py:431
  47.9 1.5 %collective-permute-done.7 = bf16[128,2048]{1,0:T(8,128)(2,1)S(1)} collective-permute-done((bf16[128,2048]{1,0:T(8,128)(2,1)S(1)}, bf16[128,2048]{1,0:T(8,128)(2,1)S(1)}, u32[]{:S(2)}, u32[]{:S(2)}) %collective-permute-start.7) | collective-permute-done | bytes 524320 | tf_op jit(solution)/shard_map/ppermute | solution.py:468
  49.7 1.7 %collective-permute-start.13 = (bf16[16,2048]{1,0:T(8,128)(2,1)S(1)}, bf16[16,2048]{1,0:T(8,128)(2,1)S(1)}, u32[]{:S(2)}, u32[]{:S(2)}) collective-permute-start(bf16[16,2048]{1,0:T(8,128)(2,1)S(1)} %get-tuple-element.28), channel_id=1, source_target_pairs={{0,6},{1,7},{2,4},{3,5},{4,2},{5,3},{6,0},{7,1},{8,14},{9,15},{10,... | collective-permute-start | bytes 196616 | tf_op jit(solution)/shard_map/ppermute | solution.py:464
  51.9 1.3 %collective-permute-start.11 = (bf16[16,2048]{1,0:T(8,128)(2,1)S(1)}, bf16[16,2048]{1,0:T(8,128)(2,1)S(1)}, u32[]{:S(2)}, u32[]{:S(2)}) collective-permute-start(bf16[16,2048]{1,0:T(8,128)(2,1)S(1)} %get-tuple-element.30), channel_id=1, source_target_pairs={{0,4},{1,3},{2,6},{3,1},{4,0},{5,7},{6,2},{7,5},{8,12},{9,11},{10,... | collective-permute-start | bytes 196616 | tf_op jit(solution)/shard_map/ppermute | solution.py:464
  53.2 0.7 %collective-permute-start.8 = (bf16[16,2048]{1,0:T(8,128)(2,1)S(1)}, bf16[16,2048]{1,0:T(8,128)(2,1)S(1)}, u32[]{:S(2)}, u32[]{:S(2)}) collective-permute-start(bf16[16,2048]{1,0:T(8,128)(2,1)S(1)} %get-tuple-element.27), channel_id=1, source_target_pairs={{0,4},{1,3},{2,6},{3,1},{4,0},{5,7},{6,2},{7,5},{8,12},{9,11},{10,... | collective-permute-start | bytes 196616 | tf_op jit(solution)/shard_map/ppermute | solution.py:464
  53.9 2.3 %collective-permute-start.10 = (bf16[16,2048]{1,0:T(8,128)(2,1)S(1)}, bf16[16,2048]{1,0:T(8,128)(2,1)S(1)}, u32[]{:S(2)}, u32[]{:S(2)}) collective-permute-start(bf16[16,2048]{1,0:T(8,128)(2,1)S(1)} %get-tuple-element.31), channel_id=1, source_target_pairs={{0,6},{1,7},{2,4},{3,5},{4,2},{5,3},{6,0},{7,1},{8,14},{9,15},{10,... | collective-permute-start | bytes 196616 | tf_op jit(solution)/shard_map/ppermute | solution.py:464
  56.2 0.9 %collective-permute-start.9 = (bf16[16,2048]{1,0:T(8,128)(2,1)S(1)}, bf16[16,2048]{1,0:T(8,128)(2,1)S(1)}, u32[]{:S(2)}, u32[]{:S(2)}) collective-permute-start(bf16[16,2048]{1,0:T(8,128)(2,1)S(1)} %get-tuple-element.32), channel_id=1, source_target_pairs={{0,2},{1,5},{2,0},{3,7},{4,6},{5,1},{6,4},{7,3},{8,10},{9,13},{10,... | collective-permute-start | bytes 196616 | tf_op jit(solution)/shard_map/ppermute | solution.py:464
  57.1 1.8 %collective-permute-start.14 = (bf16[16,2048]{1,0:T(8,128)(2,1)S(1)}, bf16[16,2048]{1,0:T(8,128)(2,1)S(1)}, u32[]{:S(2)}, u32[]{:S(2)}) collective-permute-start(bf16[16,2048]{1,0:T(8,128)(2,1)S(1)} %fusion.2), channel_id=1, source_target_pairs={{0,8},{1,17},{2,10},{3,19},{4,12},{5,21},{6,14},{7,23},{8,0},{9,25... | collective-permute-start | bytes 196616 | tf_op jit(solution)/shard_map/ppermute | solution.py:464
  59.3 1.2 %collective-permute-done.9 = bf16[16,2048]{1,0:T(8,128)(2,1)S(1)} collective-permute-done((bf16[16,2048]{1,0:T(8,128)(2,1)S(1)}, bf16[16,2048]{1,0:T(8,128)(2,1)S(1)}, u32[]{:S(2)}, u32[]{:S(2)}) %collective-permute-start.9) | collective-permute-done | bytes 65568 | tf_op jit(solution)/shard_map/ppermute | solution.py:464
  60.5 1.0 %collective-permute-done.14 = bf16[16,2048]{1,0:T(8,128)(2,1)S(1)} collective-permute-done((bf16[16,2048]{1,0:T(8,128)(2,1)S(1)}, bf16[16,2048]{1,0:T(8,128)(2,1)S(1)}, u32[]{:S(2)}, u32[]{:S(2)}) %collective-permute-start.14) | collective-permute-done | bytes 65568 | tf_op jit(solution)/shard_map/ppermute | solution.py:464
  61.5 2.8 %collective-permute-start.15 = (bf16[8,2048]{1,0:T(8,128)(2,1)S(1)}, bf16[8,2048]{1,0:T(8,128)(2,1)S(1)}, u32[]{:S(2)}, u32[]{:S(2)}) collective-permute-start(bf16[8,2048]{1,0:T(8,128)(2,1)S(1)} %slice.77), channel_id=1, source_target_pairs={{0,16},{1,9},{2,18},{3,11},{4,20},{5,13},{6,22},{7,15},{8,24},{9,1... | collective-permute-start | bytes 98312 | tf_op jit(solution)/shard_map/ppermute | solution.py:464
  64.4 2.0 %collective-permute-done.15 = bf16[8,2048]{1,0:T(8,128)(2,1)S(1)} collective-permute-done((bf16[8,2048]{1,0:T(8,128)(2,1)S(1)}, bf16[8,2048]{1,0:T(8,128)(2,1)S(1)}, u32[]{:S(2)}, u32[]{:S(2)}) %collective-permute-start.15) | collective-permute-done | bytes 32800 | tf_op jit(solution)/shard_map/ppermute | solution.py:464
  (40 shorter events, 3.9 us)
Async XLA Ops:
  0.6 8.4 %copy-start.4 = (bf16[8,2]{0,1:T(2,128)(2,1)S(1)}, bf16[8,2]{0,1:T(2,128)(2,1)}, u32[]{:S(2)}) copy-start(bf16[8,2]{0,1:T(2,128)(2,1)} %param.39) | copy-start | bytes 100
  0.6 8.5 %copy-start.3 = (s32[8,2]{0,1:T(2,128)S(1)}, s32[8,2]{0,1:T(2,128)}, u32[]{:S(2)}) copy-start(s32[8,2]{0,1:T(2,128)} %param.38) | copy-start | bytes 196
  0.7 8.6 %copy-start.2 = (bf16[2048]{0:T(1024)(128)(2,1)S(1)}, bf16[2048]{0:T(1024)(128)(2,1)}, u32[]{:S(2)}) copy-start(bf16[2048]{0:T(1024)(128)(2,1)} %param.37) | copy-start | bytes 12292
  0.7 9.2 %copy-start = (bf16[16,2048]{1,0:T(8,128)(2,1)S(1)}, bf16[16,2048]{1,0:T(8,128)(2,1)}, u32[]{:S(2)}) copy-start(bf16[16,2048]{1,0:T(8,128)(2,1)} %tokens_ref.1) | copy-start | bytes 196612
  0.7 9.2 %copy-start.1 = (f32[2048]{0:T(1024)S(1)}, f32[2048]{0:T(1024)}, u32[]{:S(2)}) copy-start(f32[2048]{0:T(1024)} %param.30) | copy-start | bytes 24580
  8.5 1.4 %collective-permute-start = (bf16[8,2048]{1,0:T(8,128)(2,1)S(1)}, bf16[8,2048]{1,0:T(8,128)(2,1)S(1)}, u32[]{:S(2)}, u32[]{:S(2)}) collective-permute-start(bf16[8,2048]{1,0:T(8,128)(2,1)S(1)} %get-tuple-element.15), channel_id=1, source_target_pairs={{0,1},{1,0},{2,3},{3,2},{4,5},{5,4},{6,7},{7,6},{8,9},{9,8},{10,11... | collective-permute-start | bytes 98312 | tf_op jit(solution)/shard_map/ppermute | solution.py:468
  10.1 5.9 %collective-permute-start.1 = (bf16[8,2176]{1,0:T(8,128)(2,1)S(1)}, bf16[8,2176]{1,0:T(8,128)(2,1)S(1)}, u32[]{:S(2)}, u32[]{:S(2)}) collective-permute-start(bf16[8,2176]{1,0:T(8,128)(2,1)S(1)} %get-tuple-element.17.refs_0_), channel_id=1, source_target_pairs={{0,16},{1,9},{2,18},{3,11},{4,20},{5,13},{6,22},{7,15},{8,24},{9,1... | collective-permute-start | bytes 104456 | tf_op jit(solution)/shard_map/ppermute | solution.py:464
  16.1 4.4 %collective-permute-start.2 = (bf16[16,2176]{1,0:T(8,128)(2,1)S(1)}, bf16[16,2176]{1,0:T(8,128)(2,1)S(1)}, u32[]{:S(2)}, u32[]{:S(2)}) collective-permute-start(bf16[16,2176]{1,0:T(8,128)(2,1)S(1)} %get-tuple-element.45.refs_0_), channel_id=1, source_target_pairs={{0,8},{1,17},{2,10},{3,19},{4,12},{5,21},{6,14},{7,23},{8,0},{9,25... | collective-permute-start | bytes 208904 | tf_op jit(solution)/shard_map/ppermute | solution.py:464
  20.5 9.2 %collective-permute-start.3 = (bf16[32,2176]{1,0:T(8,128)(2,1)S(1)}, bf16[32,2176]{1,0:T(8,128)(2,1)S(1)}, u32[]{:S(2)}, u32[]{:S(2)}) collective-permute-start(bf16[32,2176]{1,0:T(8,128)(2,1)S(1)} %get-tuple-element.41.refs_0_), channel_id=1, source_target_pairs={{0,4},{1,3},{2,6},{3,1},{4,0},{5,7},{6,2},{7,5},{8,12},{9,11},{10,... | collective-permute-start | bytes 417800 | tf_op jit(solution)/shard_map/ppermute | solution.py:464
  22.4 7.4 %collective-permute-start.5 = (bf16[32,2176]{1,0:T(8,128)(2,1)S(1)}, bf16[32,2176]{1,0:T(8,128)(2,1)S(1)}, u32[]{:S(2)}, u32[]{:S(2)}) collective-permute-start(bf16[32,2176]{1,0:T(8,128)(2,1)S(1)} %get-tuple-element.41.refs_0_), channel_id=1, source_target_pairs={{0,6},{1,7},{2,4},{3,5},{4,2},{5,3},{6,0},{7,1},{8,14},{9,15},{10,... | collective-permute-start | bytes 417800 | tf_op jit(solution)/shard_map/ppermute | solution.py:464
  23.8 5.9 %collective-permute-start.4 = (bf16[32,2176]{1,0:T(8,128)(2,1)S(1)}, bf16[32,2176]{1,0:T(8,128)(2,1)S(1)}, u32[]{:S(2)}, u32[]{:S(2)}) collective-permute-start(bf16[32,2176]{1,0:T(8,128)(2,1)S(1)} %get-tuple-element.41.refs_0_), channel_id=1, source_target_pairs={{0,2},{1,5},{2,0},{3,7},{4,6},{5,1},{6,4},{7,3},{8,10},{9,13},{10,... | collective-permute-start | bytes 417800 | tf_op jit(solution)/shard_map/ppermute | solution.py:464
  29.8 10.6 %collective-permute-start.6 = (bf16[128,2176]{1,0:T(8,128)(2,1)S(1)}, bf16[128,2176]{1,0:T(8,128)(2,1)S(1)}, u32[]{:S(2)}, u32[]{:S(2)}) collective-permute-start(bf16[128,2176]{1,0:T(8,128)(2,1)S(1)} %get-tuple-element.33), channel_id=1, source_target_pairs={{0,1},{1,0},{2,3},{3,2},{4,5},{5,4},{6,7},{7,6},{8,9},{9,8},{10,11... | collective-permute-start | bytes 1671176 | tf_op jit(solution)/shard_map/ppermute | solution.py:468
  47.3 2.2 %collective-permute-start.7 = (bf16[128,2048]{1,0:T(8,128)(2,1)S(1)}, bf16[128,2048]{1,0:T(8,128)(2,1)S(1)}, u32[]{:S(2)}, u32[]{:S(2)}) collective-permute-start(bf16[128,2048]{1,0:T(8,128)(2,1)S(1)} %get-tuple-element.22), channel_id=1, source_target_pairs={{0,1},{1,0},{2,3},{3,2},{4,5},{5,4},{6,7},{7,6},{8,9},{9,8},{10,11... | collective-permute-start | bytes 1572872 | tf_op jit(solution)/shard_map/ppermute | solution.py:468
  49.7 6.5 %collective-permute-start.13 = (bf16[16,2048]{1,0:T(8,128)(2,1)S(1)}, bf16[16,2048]{1,0:T(8,128)(2,1)S(1)}, u32[]{:S(2)}, u32[]{:S(2)}) collective-permute-start(bf16[16,2048]{1,0:T(8,128)(2,1)S(1)} %get-tuple-element.28), channel_id=1, source_target_pairs={{0,6},{1,7},{2,4},{3,5},{4,2},{5,3},{6,0},{7,1},{8,14},{9,15},{10,... | collective-permute-start | bytes 196616 | tf_op jit(solution)/shard_map/ppermute | solution.py:464
  51.3 5.7 %collective-permute-start.12 = (bf16[16,2048]{1,0:T(8,128)(2,1)S(1)}, bf16[16,2048]{1,0:T(8,128)(2,1)S(1)}, u32[]{:S(2)}, u32[]{:S(2)}) collective-permute-start(bf16[16,2048]{1,0:T(8,128)(2,1)S(1)} %get-tuple-element.29), channel_id=1, source_target_pairs={{0,2},{1,5},{2,0},{3,7},{4,6},{5,1},{6,4},{7,3},{8,10},{9,13},{10,... | collective-permute-start | bytes 196616 | tf_op jit(solution)/shard_map/ppermute | solution.py:464
  51.9 5.2 %collective-permute-start.11 = (bf16[16,2048]{1,0:T(8,128)(2,1)S(1)}, bf16[16,2048]{1,0:T(8,128)(2,1)S(1)}, u32[]{:S(2)}, u32[]{:S(2)}) collective-permute-start(bf16[16,2048]{1,0:T(8,128)(2,1)S(1)} %get-tuple-element.30), channel_id=1, source_target_pairs={{0,4},{1,3},{2,6},{3,1},{4,0},{5,7},{6,2},{7,5},{8,12},{9,11},{10,... | collective-permute-start | bytes 196616 | tf_op jit(solution)/shard_map/ppermute | solution.py:464
  53.2 6.0 %collective-permute-start.8 = (bf16[16,2048]{1,0:T(8,128)(2,1)S(1)}, bf16[16,2048]{1,0:T(8,128)(2,1)S(1)}, u32[]{:S(2)}, u32[]{:S(2)}) collective-permute-start(bf16[16,2048]{1,0:T(8,128)(2,1)S(1)} %get-tuple-element.27), channel_id=1, source_target_pairs={{0,4},{1,3},{2,6},{3,1},{4,0},{5,7},{6,2},{7,5},{8,12},{9,11},{10,... | collective-permute-start | bytes 196616 | tf_op jit(solution)/shard_map/ppermute | solution.py:464
  53.9 5.4 %collective-permute-start.10 = (bf16[16,2048]{1,0:T(8,128)(2,1)S(1)}, bf16[16,2048]{1,0:T(8,128)(2,1)S(1)}, u32[]{:S(2)}, u32[]{:S(2)}) collective-permute-start(bf16[16,2048]{1,0:T(8,128)(2,1)S(1)} %get-tuple-element.31), channel_id=1, source_target_pairs={{0,6},{1,7},{2,4},{3,5},{4,2},{5,3},{6,0},{7,1},{8,14},{9,15},{10,... | collective-permute-start | bytes 196616 | tf_op jit(solution)/shard_map/ppermute | solution.py:464
  56.2 4.3 %collective-permute-start.9 = (bf16[16,2048]{1,0:T(8,128)(2,1)S(1)}, bf16[16,2048]{1,0:T(8,128)(2,1)S(1)}, u32[]{:S(2)}, u32[]{:S(2)}) collective-permute-start(bf16[16,2048]{1,0:T(8,128)(2,1)S(1)} %get-tuple-element.32), channel_id=1, source_target_pairs={{0,2},{1,5},{2,0},{3,7},{4,6},{5,1},{6,4},{7,3},{8,10},{9,13},{10,... | collective-permute-start | bytes 196616 | tf_op jit(solution)/shard_map/ppermute | solution.py:464
  57.1 4.3 %collective-permute-start.14 = (bf16[16,2048]{1,0:T(8,128)(2,1)S(1)}, bf16[16,2048]{1,0:T(8,128)(2,1)S(1)}, u32[]{:S(2)}, u32[]{:S(2)}) collective-permute-start(bf16[16,2048]{1,0:T(8,128)(2,1)S(1)} %fusion.2), channel_id=1, source_target_pairs={{0,8},{1,17},{2,10},{3,19},{4,12},{5,21},{6,14},{7,23},{8,0},{9,25... | collective-permute-start | bytes 196616 | tf_op jit(solution)/shard_map/ppermute | solution.py:464
  61.5 4.9 %collective-permute-start.15 = (bf16[8,2048]{1,0:T(8,128)(2,1)S(1)}, bf16[8,2048]{1,0:T(8,128)(2,1)S(1)}, u32[]{:S(2)}, u32[]{:S(2)}) collective-permute-start(bf16[8,2048]{1,0:T(8,128)(2,1)S(1)} %slice.77), channel_id=1, source_target_pairs={{0,16},{1,9},{2,18},{3,11},{4,20},{5,13},{6,22},{7,15},{8,24},{9,1... | collective-permute-start | bytes 98312 | tf_op jit(solution)/shard_map/ppermute | solution.py:464

commit v3 on v2

--- a/solution.py
+++ b/solution.py
@@ -12,6 +12,7 @@
 EXPERTS = 8
 LANES = 128
 BLOCK = 256
+LAST = 1
 EPSILON = 1e-06
 FETCH_FLOPS = 200
 IN_FLIGHT = 8
@@ -339,7 +340,7 @@
     width, units = expert_gate.shape
     blocks = units // BLOCK
     early = 1
-    joined = units % BLOCK == 0 and blocks > early
+    joined = units % BLOCK == 0 and blocks > early + LAST
     dense_units = dense_gate_w.shape[1] // lax.axis_size("tp")
 
     def first_plan(sources, targets):
@@ -359,9 +360,11 @@
             for i in range(2)
         ]
 
+    cut = blocks - LAST
+
     def third_plan(sources, targets):
         if joined:
-            return wide_plan(early, blocks - early, *sources, targets[0])
+            return wide_plan(early, cut - early, *sources, targets[0])
         return [(sources[1], targets[0].at[0])]
 
     dense, dense_down, first_wide = fetch(
@@ -374,16 +377,22 @@
         3 + (2 * early if joined else 1), first_plan,
     )
     down, = fetch(after[1], (expert_down,), ((units, width),), 2, second_plan)
-    last_wide, = fetch(
+    wides = [first_wide]
+    wides += fetch(
         after[2], (expert_gate, expert_up),
-        ((blocks - early, width, 2 * BLOCK) if joined else (1, width, units),),
-        2 * (blocks - early) if joined else 1, third_plan,
-    )
-    return first_wide, last_wide, dense, down, dense_down
-
-
-def ffn_kernel(members, out_block, rows_ref, first_wide, last_wide, dense, down, dense_down,
-               own_ref, other_ref, hidden_ref):
+        ((cut - early, width, 2 * BLOCK) if joined else (1, width, units),),
+        2 * (cut - early) if joined else 1, third_plan,
+    )
+    if joined:
+        wides += fetch(
+            after[3], (expert_gate, expert_up), ((LAST, width, 2 * BLOCK),),
+            2 * LAST, lambda sources, targets: wide_plan(cut, LAST, *sources, targets[0]),
+        )
+    return (dense, down, dense_down, *wides)
+
+
+def ffn_kernel(members, out_block, rows_ref, dense, down, dense_down, *refs):
+    wides, (own_ref, other_ref, hidden_ref) = refs[:-3], refs[-3:]
     count, padded = rows_ref.shape
     width = padded - LANES
     units = down.shape[0]
@@ -399,15 +408,13 @@
         return (gate / (1.0 + jnp.exp(-gate)) * up * scale).astype(BF16)
 
     rows = rows_ref[:, :width]
-    if first_wide.shape[2] == units:
-        gate = jnp.dot(rows, first_wide[0], preferred_element_type=F32)
-        up = jnp.dot(rows, last_wide[0], preferred_element_type=F32)
+    if wides[0].shape[2] == units:
+        gate, up = (jnp.dot(rows, wide[0], preferred_element_type=F32) for wide in wides)
         hidden_ref[...] = activate(gate, up, share)
     else:
-        early = first_wide.shape[0]
-        for i in range(units // BLOCK):
-            weights = first_wide[i] if i < early else last_wide[i - early]
-            both = jnp.dot(rows, weights, preferred_element_type=F32)
+        weights = [wide.at[i] for wide in wides for i in range(wide.shape[0])]
+        for i, weight in enumerate(weights):
+            both = jnp.dot(rows, weight[...], preferred_element_type=F32)
             hidden_ref[:, i * BLOCK:(i + 1) * BLOCK] = activate(
                 both[:, :BLOCK], both[:, BLOCK:], share
             )
@@ -427,14 +434,14 @@
 def feed_forward(rows, weights, members):
     count, padded = rows.shape
     width = padded - LANES
-    units = weights[3].shape[0]
+    units = weights[1].shape[0]
     return pl.pallas_call(
         functools.partial(ffn_kernel, members, 512 if width % 512 == 0 else width),
         out_shape=(
             jax.ShapeDtypeStruct((count // 2, width), F32),
             jax.ShapeDtypeStruct((count // 2, width), BF16),
         ),
-        in_specs=[VMEM] * 6,
+        in_specs=[VMEM] * (1 + len(weights)),
         out_specs=(VMEM,) * 2,
         scratch_shapes=[pltpu.VMEM((count, units), BF16)],
         cost_estimate=pl.CostEstimate(
@@ -447,13 +454,13 @@
 
 def phases_of(n_ep):
     bits = [1 << b for b in range(n_ep.bit_length() - 1)]
-    doublings = []
-    while len(bits) >= 4:
-        high, low = bits.pop(), bits.pop()
-        doublings += [(high, low), (low, high)]
-    doublings += [(bit, bit) for bit in bits[2:]]
-    direct = [(2, 1), (1, 2), (3, 3)] if len(bits) >= 2 else [(bit, bit) for bit in bits]
-    return doublings, direct
+    if len(bits) < 4:
+        doublings = [(bit, bit) for bit in bits[2:]]
+        direct = [(1, 2), (2, 1), (3, 3)] if len(bits) >= 2 else [(bit, bit) for bit in bits]
+        return doublings, direct
+    high, low = bits[-1], bits[-2]
+    doublings = list(zip(bits[:1:-1], [2, 1] + bits[2:-2]))
+    return doublings, [(2, high | low), (1, low), (3, high)]
 
 
 def exchange(array, masks, n_ep, n_tp):
@@ -491,12 +498,13 @@
     pieces = [rows]
     for masks in direct:
         pieces.append(exchange(rows, masks, n_ep, n_tp))
+    rows = jnp.concatenate(pieces, axis=0)
     weights = fetch_weights(
-        (held[-2], held[-1], rows), expert_gate, expert_up, expert_down, dense_gate_w,
+        (held[-2], held[-1], pieces[0], rows), expert_gate, expert_up, expert_down, dense_gate_w,
         dense_up_w, dense_down_w,
     )
-    rows = jnp.concatenate(pieces, axis=0)
-    rows = jnp.concatenate([rows, swap(rows, n_tp)], axis=0)
+    got = swap(rows, n_tp)
+    rows = jnp.concatenate([rows, got], axis=0)
     own, other = feed_forward(rows, weights, n_ep * n_tp // EXPERTS)
     total = own + swap(other, n_tp).astype(F32)
     part = total.shape[0] // (2 * (len(direct) + 1))

time: 67.2 us -> 67.8 us (level)
  Pallas kernels: 25.3 us -> 26.3 us
  starting transfers between devices: 22.8 us -> 22 us
    pallas_call x3 -> x4, Pallas kernels: 10.5 us -> 11.4 us  [fetch(): pl.pallas_call(functools.partial(fetch_kernel, plan, len(arrays)), out_sh...]
    ppermute x13, starting transfers between devices: 21.5 us -> 20.7 us  [exchange(): return lax.ppermute(array, ('ep', 'tp'), pairs)]
  transfers between devices with their start and end apart: 16 -> 16, of which waited for: 9 -> 11; matrix products, arithmetic and copies ran while one was open for 0% -> 0% of each run, Pallas kernels for 16% -> 17%
where the time goes in v3:
time: 67.8 us; the launch traced here: 67.7 us
  Pallas kernels  26.3 us (39%)
  starting transfers between devices  22 us (32%)
  waiting for transfers between devices  17.4 us (26%)
  other arithmetic  0.85 us (1%)
  between operations  0.82 us (1%)
    ppermute x13, starting transfers between devices, exchange(): return lax.ppermute(array, ('ep', 'tp'), pairs)  20.7 us
    ppermute x13, waiting for transfers between devices, exchange(): return lax.ppermute(array, ('ep', 'tp'), pairs)  15.2 us
    pallas_call x4, Pallas kernels, fetch(): pl.pallas_call(functools.partial(fetch_kernel, plan, len(arrays)), out_sh...  11.4 us
    pallas_call x1, Pallas kernels, attention(): pl.pallas_call(functools.partial(attention_kernel, row_count, group, q_pa...  7.79 us
    pallas_call x1, Pallas kernels, feed_forward(): pl.pallas_call(functools.partial(ffn_kernel, members, 512 if width % 512...  6.8 us
    ppermute x3, waiting for transfers between devices, swap(): return lax.ppermute(array, 'tp', [(i, i ^ 1) for i in range(n_tp)])  2.2 us
  transfers between devices with their start and end apart: 16, of which 11 were waited for; matrix products, arithmetic and copies ran while one was open for 0% of the time, Pallas kernels for 17%

profile of v3, /device:TPU:0, one launch (start us, length us, event | category | flops | bytes accessed | tf_op | source)
XLA Modules:
  0.0 67.7 jit_solution(1896857062914186317)
XLA Ops:
  0.7 7.8 %attention.1 = (bf16[8,2048]{1,0:T(8,128)(2,1)S(1)}, bf16[8,2048]{1,0:T(8,128)(2,1)S(1)}, bf16[16,128]{1,0:T(8,128)(2,1)}, bf16[16,128]{1,0:T(8,128)(2,1)}) custom-call(s32[16]{0:T(128)} %lengths_hbm.1, bf16[16,2048]{1,0:T(8,128)(2,1)} %tokens_ref.1, f32[1,2048]{1,0:T(1,128)} %bitcast.7, f32[16]{0:T(128)} %bias_hbm.1, bf16[2048,1024]{1,0:T(8,128)(2,1)} %wq_hbm.1, ...), custom_call_target="tpu_custom_call" | custom-call | tf_op jit(solution)/shard_map/attention/pallas_call | solution.py:229
  9.2 0.7 collective-permute-done.got_ref
  10.1 4.0 %collective-permute-start.1 = (bf16[8,2176]{1,0:T(8,128)(2,1)S(1)}, bf16[8,2176]{1,0:T(8,128)(2,1)S(1)}, u32[]{:S(2)}, u32[]{:S(2)}) collective-permute-start(bf16[8,2176]{1,0:T(8,128)(2,1)S(1)} %get-tuple-element.17.refs_0_), channel_id=1, source_target_pairs={{0,16},{1,5},{2,18},{3,7},{4,20},{5,1},{6,22},{7,3},{8,24},{9,13},... | collective-permute-start | bytes 104456 | tf_op jit(solution)/shard_map/ppermute | solution.py:471
  14.1 1.9 %collective-permute-done.1 = bf16[8,2176]{1,0:T(8,128)(2,1)S(1)} collective-permute-done((bf16[8,2176]{1,0:T(8,128)(2,1)S(1)}, bf16[8,2176]{1,0:T(8,128)(2,1)S(1)}, u32[]{:S(2)}, u32[]{:S(2)}) %collective-permute-start.1) | collective-permute-done | bytes 34848 | tf_op jit(solution)/shard_map/ppermute | solution.py:471
  16.1 2.0 %collective-permute-start.2 = (bf16[16,2176]{1,0:T(8,128)(2,1)S(1)}, bf16[16,2176]{1,0:T(8,128)(2,1)S(1)}, u32[]{:S(2)}, u32[]{:S(2)}) collective-permute-start(bf16[16,2176]{1,0:T(8,128)(2,1)S(1)} %get-tuple-element.45.refs_0_), channel_id=1, source_target_pairs={{0,8},{1,3},{2,10},{3,1},{4,12},{5,7},{6,14},{7,5},{8,0},{9,11},{1... | collective-permute-start | bytes 208904 | tf_op jit(solution)/shard_map/ppermute | solution.py:471
  18.0 2.4 %collective-permute-done.2 = bf16[16,2176]{1,0:T(8,128)(2,1)S(1)} collective-permute-done((bf16[16,2176]{1,0:T(8,128)(2,1)S(1)}, bf16[16,2176]{1,0:T(8,128)(2,1)S(1)}, u32[]{:S(2)}, u32[]{:S(2)}) %collective-permute-start.2) | collective-permute-done | bytes 69664 | tf_op jit(solution)/shard_map/ppermute | solution.py:471
  20.5 1.9 %collective-permute-start.3 = (bf16[32,2176]{1,0:T(8,128)(2,1)S(1)}, bf16[32,2176]{1,0:T(8,128)(2,1)S(1)}, u32[]{:S(2)}, u32[]{:S(2)}) collective-permute-start(bf16[32,2176]{1,0:T(8,128)(2,1)S(1)} %get-tuple-element.41.refs_0_), channel_id=1, source_target_pairs={{0,4},{1,25},{2,6},{3,27},{4,0},{5,29},{6,2},{7,31},{8,12},{9,17},... | collective-permute-start | bytes 417800 | tf_op jit(solution)/shard_map/ppermute | solution.py:471
  22.4 1.4 %collective-permute-start.5 = (bf16[32,2176]{1,0:T(8,128)(2,1)S(1)}, bf16[32,2176]{1,0:T(8,128)(2,1)S(1)}, u32[]{:S(2)}, u32[]{:S(2)}) collective-permute-start(bf16[32,2176]{1,0:T(8,128)(2,1)S(1)} %get-tuple-element.41.refs_0_), channel_id=1, source_target_pairs={{0,6},{1,17},{2,4},{3,19},{4,2},{5,21},{6,0},{7,23},{8,14},{9,25},... | collective-permute-start | bytes 417800 | tf_op jit(solution)/shard_map/ppermute | solution.py:471
  24.0 2.5 %collective-permute-done.3 = bf16[32,2176]{1,0:T(8,128)(2,1)S(1)} collective-permute-done((bf16[32,2176]{1,0:T(8,128)(2,1)S(1)}, bf16[32,2176]{1,0:T(8,128)(2,1)S(1)}, u32[]{:S(2)}, u32[]{:S(2)}) %collective-permute-start.3) | collective-permute-done | bytes 139296 | tf_op jit(solution)/shard_map/ppermute | solution.py:471
  26.5 2.4 %collective-permute-done.4 = bf16[32,2176]{1,0:T(8,128)(2,1)S(1)} collective-permute-done((bf16[32,2176]{1,0:T(8,128)(2,1)S(1)}, bf16[32,2176]{1,0:T(8,128)(2,1)S(1)}, u32[]{:S(2)}, u32[]{:S(2)}) %collective-permute-start.4) | collective-permute-done | bytes 139296 | tf_op jit(solution)/shard_map/ppermute | solution.py:471
  29.0 2.4 %shard_map.211 = (bf16[2,224,2048]{2,1,0:T(8,128)(2,1)S(1)}, bf16[224,2048]{1,0:T(8,128)(2,1)S(1)}, bf16[1,2048,512]{2,1,0:T(8,128)(2,1)S(1)}) custom-call(bf16[8,2176]{1,0:T(8,128)(2,1)S(1)} %get-tuple-element.17.refs_0_, bf16[448,2048]{1,0:T(8,128)(2,1)} %bitcast.5, bf16[448,2048]{1,0:T(8,128)(2,1)} %bitcast.6, bf16[448,2048]{1,0:T(8,128)(2,1)} %refs_3_.1, ...), custom_call_target="tpu_custom_call" | custom-call | flops 969932800 | bytes 4849664 | tf_op jit(solution)/shard_map/pallas_call | solution.py:316
  31.5 3.2 %shard_map.212.down = bf16[1792,2048]{1,0:T(8,128)(2,1)S(1)} custom-call(bf16[16,2176]{1,0:T(8,128)(2,1)S(1)} %get-tuple-element.45.refs_0_, bf16[1792,2048]{1,0:T(8,128)(2,1)} %refs_1_.3), custom_call_target="tpu_custom_call" | custom-call | flops 1468006400 | bytes 7340032 | tf_op jit(solution)/shard_map/pallas_call | solution.py:316
  34.6 4.2 %shard_map.213.refs_1_ = bf16[5,2048,512]{2,1,0:T(8,128)(2,1)S(1)} custom-call(bf16[32,2176]{1,0:T(8,128)(2,1)S(1)} %get-tuple-element.41.refs_0_, bf16[2048,1792]{1,0:T(8,128)(2,1)} %refs_1_.5, bf16[2048,1792]{1,0:T(8,128)(2,1)} %refs_2_.3), custom_call_target="tpu_custom_call" | custom-call | flops 2097152000 | bytes 10485760 | tf_op jit(solution)/shard_map/pallas_call | solution.py:316
  38.9 1.6 %shard_map.214.refs_2_ = bf16[1,2048,512]{2,1,0:T(8,128)(2,1)S(1)} custom-call(bf16[128,2176]{1,0:T(8,128)(2,1)S(1)} %get-tuple-element.33.refs_0_, bf16[2048,1792]{1,0:T(8,128)(2,1)} %refs_1_.5, bf16[2048,1792]{1,0:T(8,128)(2,1)} %refs_2_.3), custom_call_target="tpu_custom_call" | custom-call | flops 419430400 | bytes 2097152 | tf_op jit(solution)/shard_map/pallas_call | solution.py:316
  40.6 6.8 %feed_forward.1 = (f32[128,2048]{1,0:T(8,128)S(1)}, bf16[128,2048]{1,0:T(8,128)(2,1)S(1)}) custom-call(bf16[256,2176]{1,0:T(8,128)(2,1)S(1)} %constant_dynamic-update-slice_fusion.11.rows_ref, bf16[2,224,2048]{2,1,0:T(8,128)(2,1)S(1)} %get-tuple-element.18.dense, bf16[1792,2048]{1,0:T(8,128)(2,1)S(1)} %shard_map.212.down, ...), custom_call_target="tpu_custom_call" | custom-call | flops 5637144576 | tf_op jit(solution)/shard_map/feed_forward/pallas_call | solution.py:438
  48.0 1.5 %collective-permute-done.7 = bf16[128,2048]{1,0:T(8,128)(2,1)S(1)} collective-permute-done((bf16[128,2048]{1,0:T(8,128)(2,1)S(1)}, bf16[128,2048]{1,0:T(8,128)(2,1)S(1)}, u32[]{:S(2)}, u32[]{:S(2)}) %collective-permute-start.7) | collective-permute-done | bytes 524320 | tf_op jit(solution)/shard_map/ppermute | solution.py:475
  49.7 2.5 %collective-permute-start.13 = (bf16[16,2048]{1,0:T(8,128)(2,1)S(1)}, bf16[16,2048]{1,0:T(8,128)(2,1)S(1)}, u32[]{:S(2)}, u32[]{:S(2)}) collective-permute-start(bf16[16,2048]{1,0:T(8,128)(2,1)S(1)} %get-tuple-element.28), channel_id=1, source_target_pairs={{0,6},{1,17},{2,4},{3,19},{4,2},{5,21},{6,0},{7,23},{8,14},{9,25},... | collective-permute-start | bytes 196616 | tf_op jit(solution)/shard_map/ppermute | solution.py:471
  53.3 1.5 %collective-permute-start.8 = (bf16[16,2048]{1,0:T(8,128)(2,1)S(1)}, bf16[16,2048]{1,0:T(8,128)(2,1)S(1)}, u32[]{:S(2)}, u32[]{:S(2)}) collective-permute-start(bf16[16,2048]{1,0:T(8,128)(2,1)S(1)} %get-tuple-element.27), channel_id=1, source_target_pairs={{0,4},{1,25},{2,6},{3,27},{4,0},{5,29},{6,2},{7,31},{8,12},{9,17},... | collective-permute-start | bytes 196616 | tf_op jit(solution)/shard_map/ppermute | solution.py:471
  54.8 1.5 %collective-permute-start.10 = (bf16[16,2048]{1,0:T(8,128)(2,1)S(1)}, bf16[16,2048]{1,0:T(8,128)(2,1)S(1)}, u32[]{:S(2)}, u32[]{:S(2)}) collective-permute-start(bf16[16,2048]{1,0:T(8,128)(2,1)S(1)} %get-tuple-element.31), channel_id=1, source_target_pairs={{0,6},{1,17},{2,4},{3,19},{4,2},{5,21},{6,0},{7,23},{8,14},{9,25},... | collective-permute-start | bytes 196616 | tf_op jit(solution)/shard_map/ppermute | solution.py:471
  57.1 1.6 %collective-permute-start.14 = (bf16[16,2048]{1,0:T(8,128)(2,1)S(1)}, bf16[16,2048]{1,0:T(8,128)(2,1)S(1)}, u32[]{:S(2)}, u32[]{:S(2)}) collective-permute-start(bf16[16,2048]{1,0:T(8,128)(2,1)S(1)} %fusion.2), channel_id=1, source_target_pairs={{0,8},{1,3},{2,10},{3,1},{4,12},{5,7},{6,14},{7,5},{8,0},{9,11},{1... | collective-permute-start | bytes 196616 | tf_op jit(solution)/shard_map/ppermute | solution.py:471
  58.7 1.2 %collective-permute-done.10 = bf16[16,2048]{1,0:T(8,128)(2,1)S(1)} collective-permute-done((bf16[16,2048]{1,0:T(8,128)(2,1)S(1)}, bf16[16,2048]{1,0:T(8,128)(2,1)S(1)}, u32[]{:S(2)}, u32[]{:S(2)}) %collective-permute-start.10) | collective-permute-done | bytes 65568 | tf_op jit(solution)/shard_map/ppermute | solution.py:471
  60.5 1.6 %collective-permute-done.14 = bf16[16,2048]{1,0:T(8,128)(2,1)S(1)} collective-permute-done((bf16[16,2048]{1,0:T(8,128)(2,1)S(1)}, bf16[16,2048]{1,0:T(8,128)(2,1)S(1)}, u32[]{:S(2)}, u32[]{:S(2)}) %collective-permute-start.14) | collective-permute-done | bytes 65568 | tf_op jit(solution)/shard_map/ppermute | solution.py:471
  62.2 2.5 %collective-permute-start.15 = (bf16[8,2048]{1,0:T(8,128)(2,1)S(1)}, bf16[8,2048]{1,0:T(8,128)(2,1)S(1)}, u32[]{:S(2)}, u32[]{:S(2)}) collective-permute-start(bf16[8,2048]{1,0:T(8,128)(2,1)S(1)} %slice.77), channel_id=1, source_target_pairs={{0,16},{1,5},{2,18},{3,7},{4,20},{5,1},{6,22},{7,3},{8,24},{9,13},... | collective-permute-start | bytes 98312 | tf_op jit(solution)/shard_map/ppermute | solution.py:471
  64.7 2.4 %collective-permute-done.15 = bf16[8,2048]{1,0:T(8,128)(2,1)S(1)} collective-permute-done((bf16[8,2048]{1,0:T(8,128)(2,1)S(1)}, bf16[8,2048]{1,0:T(8,128)(2,1)S(1)}, u32[]{:S(2)}, u32[]{:S(2)}) %collective-permute-start.15) | collective-permute-done | bytes 32800 | tf_op jit(solution)/shard_map/ppermute | solution.py:471
  (41 shorter events, 5.4 us)
Async XLA Ops:
  0.6 8.4 %copy-start.4 = (bf16[8,2]{0,1:T(2,128)(2,1)S(1)}, bf16[8,2]{0,1:T(2,128)(2,1)}, u32[]{:S(2)}) copy-start(bf16[8,2]{0,1:T(2,128)(2,1)} %param.39) | copy-start | bytes 100
  0.6 8.5 %copy-start.3 = (s32[8,2]{0,1:T(2,128)S(1)}, s32[8,2]{0,1:T(2,128)}, u32[]{:S(2)}) copy-start(s32[8,2]{0,1:T(2,128)} %param.38) | copy-start | bytes 196
  0.7 8.6 %copy-start.2 = (bf16[2048]{0:T(1024)(128)(2,1)S(1)}, bf16[2048]{0:T(1024)(128)(2,1)}, u32[]{:S(2)}) copy-start(bf16[2048]{0:T(1024)(128)(2,1)} %param.37) | copy-start | bytes 12292
  0.7 9.2 %copy-start = (bf16[16,2048]{1,0:T(8,128)(2,1)S(1)}, bf16[16,2048]{1,0:T(8,128)(2,1)}, u32[]{:S(2)}) copy-start(bf16[16,2048]{1,0:T(8,128)(2,1)} %tokens_ref.1) | copy-start | bytes 196612
  0.7 9.2 %copy-start.1 = (f32[2048]{0:T(1024)S(1)}, f32[2048]{0:T(1024)}, u32[]{:S(2)}) copy-start(f32[2048]{0:T(1024)} %param.30) | copy-start | bytes 24580
  8.5 1.4 %collective-permute-start = (bf16[8,2048]{1,0:T(8,128)(2,1)S(1)}, bf16[8,2048]{1,0:T(8,128)(2,1)S(1)}, u32[]{:S(2)}, u32[]{:S(2)}) collective-permute-start(bf16[8,2048]{1,0:T(8,128)(2,1)S(1)} %get-tuple-element.15), channel_id=1, source_target_pairs={{0,1},{1,0},{2,3},{3,2},{4,5},{5,4},{6,7},{7,6},{8,9},{9,8},{10,11... | collective-permute-start | bytes 98312 | tf_op jit(solution)/shard_map/ppermute | solution.py:475
  10.1 5.9 %collective-permute-start.1 = (bf16[8,2176]{1,0:T(8,128)(2,1)S(1)}, bf16[8,2176]{1,0:T(8,128)(2,1)S(1)}, u32[]{:S(2)}, u32[]{:S(2)}) collective-permute-start(bf16[8,2176]{1,0:T(8,128)(2,1)S(1)} %get-tuple-element.17.refs_0_), channel_id=1, source_target_pairs={{0,16},{1,5},{2,18},{3,7},{4,20},{5,1},{6,22},{7,3},{8,24},{9,13},... | collective-permute-start | bytes 104456 | tf_op jit(solution)/shard_map/ppermute | solution.py:471
  16.1 4.4 %collective-permute-start.2 = (bf16[16,2176]{1,0:T(8,128)(2,1)S(1)}, bf16[16,2176]{1,0:T(8,128)(2,1)S(1)}, u32[]{:S(2)}, u32[]{:S(2)}) collective-permute-start(bf16[16,2176]{1,0:T(8,128)(2,1)S(1)} %get-tuple-element.45.refs_0_), channel_id=1, source_target_pairs={{0,8},{1,3},{2,10},{3,1},{4,12},{5,7},{6,14},{7,5},{8,0},{9,11},{1... | collective-permute-start | bytes 208904 | tf_op jit(solution)/shard_map/ppermute | solution.py:471
  20.5 6.0 %collective-permute-start.3 = (bf16[32,2176]{1,0:T(8,128)(2,1)S(1)}, bf16[32,2176]{1,0:T(8,128)(2,1)S(1)}, u32[]{:S(2)}, u32[]{:S(2)}) collective-permute-start(bf16[32,2176]{1,0:T(8,128)(2,1)S(1)} %get-tuple-element.41.refs_0_), channel_id=1, source_target_pairs={{0,4},{1,25},{2,6},{3,27},{4,0},{5,29},{6,2},{7,31},{8,12},{9,17},... | collective-permute-start | bytes 417800 | tf_op jit(solution)/shard_map/ppermute | solution.py:471
  22.4 6.5 %collective-permute-start.5 = (bf16[32,2176]{1,0:T(8,128)(2,1)S(1)}, bf16[32,2176]{1,0:T(8,128)(2,1)S(1)}, u32[]{:S(2)}, u32[]{:S(2)}) collective-permute-start(bf16[32,2176]{1,0:T(8,128)(2,1)S(1)} %get-tuple-element.41.refs_0_), channel_id=1, source_target_pairs={{0,6},{1,17},{2,4},{3,19},{4,2},{5,21},{6,0},{7,23},{8,14},{9,25},... | collective-permute-start | bytes 417800 | tf_op jit(solution)/shard_map/ppermute | solution.py:471
  23.8 5.1 %collective-permute-start.4 = (bf16[32,2176]{1,0:T(8,128)(2,1)S(1)}, bf16[32,2176]{1,0:T(8,128)(2,1)S(1)}, u32[]{:S(2)}, u32[]{:S(2)}) collective-permute-start(bf16[32,2176]{1,0:T(8,128)(2,1)S(1)} %get-tuple-element.41.refs_0_), channel_id=1, source_target_pairs={{0,2},{1,9},{2,0},{3,11},{4,6},{5,13},{6,4},{7,15},{8,10},{9,1},{1... | collective-permute-start | bytes 417800 | tf_op jit(solution)/shard_map/ppermute | solution.py:471
  28.9 11.6 %collective-permute-start.6 = (bf16[128,2176]{1,0:T(8,128)(2,1)S(1)}, bf16[128,2176]{1,0:T(8,128)(2,1)S(1)}, u32[]{:S(2)}, u32[]{:S(2)}) collective-permute-start(bf16[128,2176]{1,0:T(8,128)(2,1)S(1)} %get-tuple-element.33.refs_0_), channel_id=1, source_target_pairs={{0,1},{1,0},{2,3},{3,2},{4,5},{5,4},{6,7},{7,6},{8,9},{9,8},{10,11... | collective-permute-start | bytes 1671176 | tf_op jit(solution)/shard_map/ppermute | solution.py:475
  47.4 2.2 %collective-permute-start.7 = (bf16[128,2048]{1,0:T(8,128)(2,1)S(1)}, bf16[128,2048]{1,0:T(8,128)(2,1)S(1)}, u32[]{:S(2)}, u32[]{:S(2)}) collective-permute-start(bf16[128,2048]{1,0:T(8,128)(2,1)S(1)} %get-tuple-element.22), channel_id=1, source_target_pairs={{0,1},{1,0},{2,3},{3,2},{4,5},{5,4},{6,7},{7,6},{8,9},{9,8},{10,11... | collective-permute-start | bytes 1572872 | tf_op jit(solution)/shard_map/ppermute | solution.py:475
  49.7 6.5 %collective-permute-start.13 = (bf16[16,2048]{1,0:T(8,128)(2,1)S(1)}, bf16[16,2048]{1,0:T(8,128)(2,1)S(1)}, u32[]{:S(2)}, u32[]{:S(2)}) collective-permute-start(bf16[16,2048]{1,0:T(8,128)(2,1)S(1)} %get-tuple-element.28), channel_id=1, source_target_pairs={{0,6},{1,17},{2,4},{3,19},{4,2},{5,21},{6,0},{7,23},{8,14},{9,25},... | collective-permute-start | bytes 196616 | tf_op jit(solution)/shard_map/ppermute | solution.py:471
  52.2 4.5 %collective-permute-start.12 = (bf16[16,2048]{1,0:T(8,128)(2,1)S(1)}, bf16[16,2048]{1,0:T(8,128)(2,1)S(1)}, u32[]{:S(2)}, u32[]{:S(2)}) collective-permute-start(bf16[16,2048]{1,0:T(8,128)(2,1)S(1)} %get-tuple-element.29), channel_id=1, source_target_pairs={{0,2},{1,9},{2,0},{3,11},{4,6},{5,13},{6,4},{7,15},{8,10},{9,1},{1... | collective-permute-start | bytes 196616 | tf_op jit(solution)/shard_map/ppermute | solution.py:471
  52.8 4.3 %collective-permute-start.11 = (bf16[16,2048]{1,0:T(8,128)(2,1)S(1)}, bf16[16,2048]{1,0:T(8,128)(2,1)S(1)}, u32[]{:S(2)}, u32[]{:S(2)}) collective-permute-start(bf16[16,2048]{1,0:T(8,128)(2,1)S(1)} %get-tuple-element.30), channel_id=1, source_target_pairs={{0,4},{1,25},{2,6},{3,27},{4,0},{5,29},{6,2},{7,31},{8,12},{9,17},... | collective-permute-start | bytes 196616 | tf_op jit(solution)/shard_map/ppermute | solution.py:471
  53.3 5.4 %collective-permute-start.8 = (bf16[16,2048]{1,0:T(8,128)(2,1)S(1)}, bf16[16,2048]{1,0:T(8,128)(2,1)S(1)}, u32[]{:S(2)}, u32[]{:S(2)}) collective-permute-start(bf16[16,2048]{1,0:T(8,128)(2,1)S(1)} %get-tuple-element.27), channel_id=1, source_target_pairs={{0,4},{1,25},{2,6},{3,27},{4,0},{5,29},{6,2},{7,31},{8,12},{9,17},... | collective-permute-start | bytes 196616 | tf_op jit(solution)/shard_map/ppermute | solution.py:471
  54.8 5.2 %collective-permute-start.10 = (bf16[16,2048]{1,0:T(8,128)(2,1)S(1)}, bf16[16,2048]{1,0:T(8,128)(2,1)S(1)}, u32[]{:S(2)}, u32[]{:S(2)}) collective-permute-start(bf16[16,2048]{1,0:T(8,128)(2,1)S(1)} %get-tuple-element.31), channel_id=1, source_target_pairs={{0,6},{1,17},{2,4},{3,19},{4,2},{5,21},{6,0},{7,23},{8,14},{9,25},... | collective-permute-start | bytes 196616 | tf_op jit(solution)/shard_map/ppermute | solution.py:471
  56.3 4.3 %collective-permute-start.9 = (bf16[16,2048]{1,0:T(8,128)(2,1)S(1)}, bf16[16,2048]{1,0:T(8,128)(2,1)S(1)}, u32[]{:S(2)}, u32[]{:S(2)}) collective-permute-start(bf16[16,2048]{1,0:T(8,128)(2,1)S(1)} %get-tuple-element.32), channel_id=1, source_target_pairs={{0,2},{1,9},{2,0},{3,11},{4,6},{5,13},{6,4},{7,15},{8,10},{9,1},{1... | collective-permute-start | bytes 196616 | tf_op jit(solution)/shard_map/ppermute | solution.py:471
  57.1 5.0 %collective-permute-start.14 = (bf16[16,2048]{1,0:T(8,128)(2,1)S(1)}, bf16[16,2048]{1,0:T(8,128)(2,1)S(1)}, u32[]{:S(2)}, u32[]{:S(2)}) collective-permute-start(bf16[16,2048]{1,0:T(8,128)(2,1)S(1)} %fusion.2), channel_id=1, source_target_pairs={{0,8},{1,3},{2,10},{3,1},{4,12},{5,7},{6,14},{7,5},{8,0},{9,11},{1... | collective-permute-start | bytes 196616 | tf_op jit(solution)/shard_map/ppermute | solution.py:471
  62.2 4.9 %collective-permute-start.15 = (bf16[8,2048]{1,0:T(8,128)(2,1)S(1)}, bf16[8,2048]{1,0:T(8,128)(2,1)S(1)}, u32[]{:S(2)}, u32[]{:S(2)}) collective-permute-start(bf16[8,2048]{1,0:T(8,128)(2,1)S(1)} %slice.77), channel_id=1, source_target_pairs={{0,16},{1,5},{2,18},{3,7},{4,20},{5,1},{6,22},{7,3},{8,24},{9,13},... | collective-permute-start | bytes 98312 | tf_op jit(solution)/shard_map/ppermute | solution.py:471
